TPU v7x, 32 devices: a whole 2x2x4 slice. The times are simulated.
32 devices in a mesh: grp: 2 (over y), dp: 2 (over x), kv: 4 (over z), tp: 2 (over core).
Axes of the slice: x: 2, y: 2, z: 4, core: 2. Of those that a mesh axis runs over, the one named last changes fastest.
Arguments:
- tokens: bfloat16 [16, 4096], P('grp', ('dp', 'kv')), parts along dimension 0, may hold values from -40 to 40
- lengths: int32 [16], P(('grp', 'dp')), parts along dimension 0, may hold values from 2 to 512, as said below
- cache_keys: bfloat16 [16, 512, 6, 256], P(('grp', 'dp'), 'kv', 'tp'), parts along dimension 0, may hold values from -6 to 6
- cache_values: bfloat16 [16, 512, 6, 512], P(('grp', 'dp'), 'kv', 'tp'), parts along dimension 0, may hold values from -6 to 6
- cache_igate: float32 [16, 6, 512], P(('grp', 'dp'), 'tp', 'kv'), parts along dimension 0, may hold values from -5 to 250
- cache_fcum: float32 [16, 6, 512], P(('grp', 'dp'), 'tp', 'kv'), parts along dimension 0, may hold values from -130 to 0, as said below
- gain_mix: bfloat16 [4096], replicated, may hold values from 0.099609375 to 1.8984375
- w_query: bfloat16 [4096, 1536], P(('dp', 'kv'), 'tp'), may hold values from -0.09375 to 0.09375
- w_key: bfloat16 [4096, 1536], P(('dp', 'kv'), 'tp'), may hold values from -0.09375 to 0.09375
- w_value: bfloat16 [4096, 3072], P(('dp', 'kv'), 'tp'), may hold values from -0.09375 to 0.09375
- w_gates: bfloat16 [4096, 12], replicated, may hold values from -0.09375 to 0.09375
- w_out: bfloat16 [3072, 4096], P(None, ('dp', 'kv', 'tp')), may hold values from -0.109375 to 0.109375
- gain_ffn: bfloat16 [4096], replicated, may hold values from 0.099609375 to 1.8984375
- w_gate: bfloat16 [4096, 10240], P(None, ('dp', 'kv', 'tp')), may hold values from -0.09375 to 0.09375
- w_up: bfloat16 [4096, 10240], P(None, ('dp', 'kv', 'tp')), may hold values from -0.09375 to 0.09375
- w_down: bfloat16 [10240, 4096], P(('dp', 'kv', 'tp')), may hold values from -0.078125 to 0.078125
Outputs:
- result: bfloat16 [16, 4096], P('grp', ('dp', 'kv', 'tp')), parts along dimension 0
There are 2 independent parts, one for each index of `grp`. A program takes and returns all parts, laid end to end along the dimension named above; an argument that names none is the same for every part. Nothing has to cross between parts.
Inputs may be any that keep to these rules, and one draw needn't show every extreme that they name: Live cache positions of each sequence; the new token takes position lengths; in every draw one sequence has exactly 512. `cache_fcum`: position p holds the sum of the log forget gates of positions 0 to p of its sequence and head; never rising along positions.
All inputs are finite; a program needn't handle non-finite values.
Results may differ from a plain program's by a relative error of at most 0.012.
Values may be sent and summed in bfloat16 or wider, within the bound.
A program may use at most 64 MiB of HBM per device.

v0:
```python
import functools

import jax
import jax.numpy as jnp
from jax import lax
from jax.experimental import pallas as pl
from jax.experimental.pallas import tpu as pltpu
from jax.sharding import PartitionSpec as P

epsilon = 1e-06
very_low = -1e30


def combined_all(value, axis, join):
    pieces = jax.tree.map(lambda part: lax.all_gather(part, axis), value)
    head = jax.tree.map(lambda part: part[0], pieces)
    tail = jax.tree.map(lambda part: part[1:], pieces)
    total, _ = lax.scan(lambda total, piece: (join(total, piece), None), head, tail)
    return total


def merge_partial(first_part, second_part):
    max_first, den_first, num_first, anchor_first = first_part
    max_second, den_second, num_second, anchor_second = second_part
    highest = jnp.maximum(max_first, max_second)
    scale_first = jnp.exp(max_first - highest)
    scale_second = jnp.exp(max_second - highest)
    denominator = scale_first * den_first + scale_second * den_second
    numerator = scale_first[..., None] * num_first + scale_second[..., None] * num_second
    return (highest, denominator, numerator, jnp.maximum(anchor_first, anchor_second))


def per_device(
    tokens,
    lengths,
    cache_keys,
    cache_values,
    cache_igate,
    cache_fcum,
    gain_mix,
    w_query,
    w_key,
    w_value,
    w_gates,
    w_out,
    gain_ffn,
    w_gate,
    w_up,
    w_down,
):
    count_dp = lax.axis_size("dp")
    count_kv = lax.axis_size("kv")
    count_tp = lax.axis_size("tp")
    index_dp = lax.axis_index("dp")
    index_kv = lax.axis_index("kv")
    index_tp = lax.axis_index("tp")
    row_count, feat_block = tokens.shape
    seq_count, block_len, head_local, key_dimension = cache_keys.shape
    value_size = cache_values.shape[3]
    model_width = gain_mix.shape[0]
    heads_total = w_gates.shape[1] // 2
    out_block = w_out.shape[1]
    col_start = (index_dp * count_kv + index_kv) * feat_block
    token_f32 = tokens.astype(jnp.float32)
    gain_part = lax.dynamic_slice_in_dim(gain_mix, col_start, feat_block, 0).astype(jnp.float32)
    scaled = (token_f32 * gain_part[None, :]).astype(jnp.bfloat16)
    energy = jnp.sum(token_f32 * token_f32, axis=1)
    joined = jnp.concatenate(
        [
            jnp.dot(scaled, w_query, preferred_element_type=jnp.float32),
            jnp.dot(scaled, w_key, preferred_element_type=jnp.float32),
            jnp.dot(scaled, w_value, preferred_element_type=jnp.float32),
        ],
        axis=1,
    )
    gate_rows = lax.dynamic_slice_in_dim(w_gates, col_start, feat_block, 0).reshape(
        feat_block, 2, heads_total
    )
    gate_cols = lax.dynamic_slice_in_dim(gate_rows, index_tp * head_local, head_local, 2).reshape(
        feat_block, 2 * head_local
    )
    gate_part = jnp.dot(scaled, gate_cols, preferred_element_type=jnp.float32)
    joined_part, gate_rowsum, energy_part = (
        lax.psum_scatter(joined, "dp", scatter_dimension=0, tiled=True),
        lax.psum_scatter(gate_part, "dp", scatter_dimension=0, tiled=True),
        lax.psum_scatter(energy, "dp", scatter_dimension=0, tiled=True),
    )
    joined_own, gate_own, energy_own = lax.psum((joined_part, gate_rowsum, energy_part), "kv")
    inv_norm = lax.rsqrt(energy_own / model_width + epsilon)[:, None]
    width_qk = head_local * key_dimension
    query_new = (
        (joined_own[:, :width_qk] * inv_norm)
        .astype(jnp.bfloat16)
        .reshape(seq_count, head_local, key_dimension)
    )
    new_key = (
        (joined_own[:, width_qk : 2 * width_qk] * inv_norm)
        .astype(jnp.bfloat16)
        .reshape(seq_count, head_local, key_dimension)
    )
    new_value = (
        (joined_own[:, 2 * width_qk :] * inv_norm)
        .astype(jnp.bfloat16)
        .reshape(seq_count, head_local, value_size)
    )
    gates_now = gate_own * inv_norm
    in_gate = gates_now[:, :head_local]
    log_forget = jax.nn.log_sigmoid(gates_now[:, head_local:])
    inv_root = key_dimension ** (-0.5)
    scores = (
        jnp.einsum("shk,sphk->shp", query_new, cache_keys, preferred_element_type=jnp.float32)
        * inv_root
    )
    positions = index_kv * block_len + jnp.arange(block_len, dtype=jnp.int32)
    is_live = positions[None, None, :] < lengths[:, None, None]
    exponent = jnp.where(is_live, cache_igate - cache_fcum, very_low)
    block_max = jnp.max(exponent, axis=2)
    weight = jnp.where(is_live, jnp.exp(exponent - block_max[..., None]), 0.0)
    product = weight * scores
    block_den = jnp.sum(product, axis=2)
    block_num = jnp.einsum(
        "shp,sphv->shv",
        product.astype(jnp.bfloat16),
        cache_values,
        preferred_element_type=jnp.float32,
    )
    holding = positions[None, None, :] == (lengths - 1)[:, None, None]
    anchor = jnp.max(jnp.where(holding, cache_fcum, very_low), axis=2)
    cache_max, cache_den, cache_num, anchor_all = combined_all(
        (block_max, block_den, block_num, anchor), "kv", merge_partial
    )
    own_score = (
        jnp.sum(query_new.astype(jnp.float32) * new_key.astype(jnp.float32), axis=2) * inv_root
    )
    own_prob = lax.optimization_barrier(own_score.astype(jnp.bfloat16)).astype(jnp.float32)
    own_num = own_prob[..., None] * new_value.astype(jnp.float32)
    carried = anchor_all + log_forget
    highest = jnp.maximum(carried + cache_max, in_gate)
    weight_cache = jnp.exp(carried + cache_max - highest)
    weight_own = jnp.exp(in_gate - highest)
    denominator = weight_cache * cache_den + weight_own * own_score
    numerator = weight_cache[..., None] * cache_num + weight_own[..., None] * own_num
    heads_out = (numerator / jnp.maximum(jnp.abs(denominator), 1.0)[..., None]).astype(jnp.bfloat16)
    heads_out = heads_out.reshape(seq_count, head_local * value_size)
    gathered = lax.all_gather(heads_out[None], ("dp", "tp"), axis=0, tiled=True)
    gathered = gathered.reshape(count_dp, count_tp, seq_count, head_local * value_size)
    out_weight = w_out.reshape(count_tp, head_local * value_size, out_block)
    attended = jnp.einsum(
        "atsk,tkc->asc", gathered, out_weight, preferred_element_type=jnp.float32
    ).reshape(row_count, out_block)
    own_cols = lax.dynamic_slice_in_dim(token_f32, index_tp * out_block, out_block, 1)
    residual = (own_cols + attended).astype(jnp.bfloat16)
    full_rows = lax.all_gather(residual, ("dp", "kv", "tp"), axis=1, tiled=True)
    full_f32 = full_rows.astype(jnp.float32)
    inv_norm_ffn = lax.rsqrt(jnp.mean(full_f32 * full_f32, axis=1, keepdims=True) + epsilon)
    normed = (full_f32 * inv_norm_ffn * gain_ffn.astype(jnp.float32)[None, :]).astype(jnp.bfloat16)
    gate_act = jnp.dot(normed, w_gate, preferred_element_type=jnp.float32)
    up_act = jnp.dot(normed, w_up, preferred_element_type=jnp.float32)
    hidden = (jax.nn.silu(gate_act) * up_act).astype(jnp.bfloat16)
    summed = lax.psum_scatter(
        lax.dot_general(
            w_down, hidden, (((0,), (1,)), ((), ())), preferred_element_type=jnp.float32
        ),
        ("dp", "kv", "tp"),
        scatter_dimension=0,
        tiled=True,
    )
    return (residual.astype(jnp.float32) + summed.T).astype(jnp.bfloat16)


def fused_kernel(
    sizes, lengths, tokens, cache_igate, cache_fcum, gain_mix, gain_ffn,
    cache_keys, cache_values, w_query, w_key, w_value, w_gates, w_out, w_gate, w_up, w_down,
    out_ref,
    wq_v, wk_v, wv_v, wg_v, wo_v, wgate_v, wup_v, wdown_v,
    keys_by_head, values_by_head,
    q_src, kv_src, small_src, q_rx, kv_rx, small_rx, small_sum, q_sum,
    part_src, part_rx, heads_rx, heads_all, resid_rx, down_src, down_rx, gains,
    load_sem, a_send, a_recv, c_send, c_recv, d_send, d_recv, e_send, e_recv, f_send, f_recv,
):
    count_dp, count_kv, count_tp = sizes
    count = count_dp * count_kv * count_tp
    blocks = count_dp * count_kv
    dp, kv, tp = lax.axis_index("dp"), lax.axis_index("kv"), lax.axis_index("tp")
    f32, bf16 = jnp.float32, jnp.bfloat16
    seqs, heads, block_len, key_size = cache_keys.shape
    value_size = cache_values.shape[3]
    rows, feat = tokens.shape
    width_q = heads * key_size
    width_v = heads * value_size
    half_kv = (width_q + width_v) // 2
    half_v = width_v // 2
    out_block = out_ref.shape[1]
    model_width = feat * blocks
    heads_total = heads * count_tp
    block = dp * count_kv + kv
    me = block * count_tp + tp

    def split(r):
        return r // (count_kv * count_tp), (r // count_tp) % count_kv, r % count_tp

    def target(r):
        a, b, c = split(r)
        return (dp + a) % count_dp, (kv + b) % count_kv, (tp + c) % count_tp

    def source(r):
        a, b, c = split(r)
        s_dp = (dp + count_dp - a) % count_dp
        s_kv = (kv + count_kv - b) % count_kv
        s_tp = (tp + count_tp - c) % count_tp
        return (s_dp * count_kv + s_kv) * count_tp + s_tp

    def device(r):
        t = target(r)
        return {"dp": t[0], "kv": t[1], "tp": t[2]}

    def distance(r):
        a, b, c = split(r)
        return (a + min(b, count_kv - b)) * 2 + c

    near = sorted(range(1, count), key=distance)

    def gain_row(which, at, width):
        lines = width // 128
        first = at * lines
        return jnp.concatenate(
            [gains[which, pl.ds(first + i, 1), :] for i in range(lines)], axis=1
        )

    def load(hbm, vmem, index, pieces=1):
        step = hbm.shape[0] // pieces
        for i in range(pieces):
            pltpu.make_async_copy(
                hbm.at[pl.ds(i * step, step)], vmem.at[pl.ds(i * step, step)], load_sem.at[index]
            ).start()

    def loaded(vmem, index):
        pltpu.make_async_copy(vmem, vmem, load_sem.at[index]).wait()

    def remote(src, dst, send, recv, where):
        copy = pltpu.make_async_remote_copy(
            src_ref=src, dst_ref=dst, send_sem=send, recv_sem=recv,
            device_id=where, device_id_type=pl.DeviceIdType.MESH,
        )
        copy.start()
        return copy

    barrier = pltpu.get_barrier_semaphore()
    for r in range(1, count):
        pl.semaphore_signal(
            barrier, inc=1, device_id=device(r), device_id_type=pl.DeviceIdType.MESH
        )
    load(w_query, wq_v, 0, 2)
    load(w_key, wk_v, 1, 2)
    load(w_value, wv_v, 2, 4)
    gate_start = pl.multiple_of(block * feat, feat)
    pltpu.make_async_copy(w_gates.at[:, pl.ds(gate_start, feat)], wg_v, load_sem.at[3]).start()
    load(cache_keys, keys_by_head, 4, seqs)
    load(cache_values, values_by_head, 5, seqs)

    gains[0] = gain_mix[...].astype(f32)
    gains[1] = gain_ffn[...].astype(f32)
    token = tokens[...].astype(f32)
    scaled = (token * gain_row(0, block, feat)).astype(bf16)
    energy = jnp.sum(token * token, axis=1, keepdims=True)
    dot = functools.partial(jnp.dot, preferred_element_type=f32)
    part_src[...] = jnp.zeros(part_src.shape, f32)
    small_src[...] = jnp.zeros(small_src.shape, f32)
    loaded(wg_v, 3)
    gate_part = lax.dot_general(
        scaled, wg_v[...], (((1,), (1,)), ((), ())), preferred_element_type=f32
    )
    for a in range(count_dp):
        small_src[a, :, 0 : 2 * heads_total] = gate_part[a * seqs : (a + 1) * seqs]
        small_src[a, :, 2 * heads_total : 2 * heads_total + 1] = energy[a * seqs : (a + 1) * seqs]
    loaded(wq_v, 0)
    query = dot(scaled, wq_v[...])
    for a in range(count_dp):
        q_src[a] = query[a * seqs : (a + 1) * seqs].astype(bf16)
    pl.semaphore_wait(barrier, count - 1)
    copies = []
    a_copies, kv_copies = [], []
    peers = sorted(range(count_tp, count, count_tp), key=distance)[::-1]
    for r in peers:
        n, to = r // count_tp, target(r)[0]
        a_copies += [
            remote(small_src.at[to], small_rx.at[n], a_send.at[1, n], a_recv.at[1, n], device(r)),
            remote(q_src.at[to], q_rx.at[n], a_send.at[0, n], a_recv.at[0, n], device(r)),
        ]
    loaded(wk_v, 1)
    key_part = dot(scaled, wk_v[...])
    loaded(wv_v, 2)
    load(w_out, wo_v, 6, 4)
    load(w_gate, wgate_v, 7, 8)
    load(w_up, wup_v, 8, 8)
    for j in range(count):
        pltpu.make_async_copy(
            w_down.at[:, pl.ds(j * out_block, out_block)], wdown_v.at[j], load_sem.at[9]
        ).start()
    value_part = dot(scaled, wv_v[...])
    joined = jnp.concatenate([key_part, value_part], axis=1)
    for i in range(rows):
        row = joined[i : i + 1]
        kv_src[i] = jnp.concatenate([row[:, :half_kv], row[:, half_kv:]], axis=0).astype(bf16)
    for r in peers:
        n, t = r // count_tp, target(r)
        kv_copies.append(
            remote(
                kv_src.at[t[0] * count_kv + t[1]],
                kv_rx.at[n], a_send.at[2, n], a_recv.at[2, n], device(r),
            )
        )

    position = kv * block_len + lax.broadcasted_iota(jnp.int32, (heads, block_len), 1)
    weights, maxes, anchors = [], [], []
    for s in range(seqs):
        live = position < lengths[s]
        fcum = cache_fcum[:, s, :]
        exponent = jnp.where(live, cache_igate[:, s, :] - fcum, very_low)
        top = jnp.max(exponent, axis=1, keepdims=True)
        weights.append(jnp.where(live, jnp.exp(exponent - top), 0.0))
        maxes.append(top)
        anchors.append(
            jnp.max(jnp.where(position == lengths[s] - 1, fcum, very_low), axis=1, keepdims=True)
        )

    for copy in a_copies:
        copy.wait_recv()
    copies.extend(a_copies)
    q_total = q_src[dp].astype(f32)
    small = small_src[dp]
    for n in range(1, blocks):
        q_total += q_rx[n].astype(f32)
        small += small_rx[n]
    small_sum[...] = small
    energies = small[:, 2 * heads_total : 2 * heads_total + 1]
    query_new = (q_total * lax.rsqrt(energies / model_width + epsilon)).astype(bf16)
    q_sum[...] = query_new.astype(f32)

    loaded(keys_by_head, 4)
    loaded(values_by_head, 5)
    inv_root = key_size ** (-0.5)
    lane = lax.broadcasted_iota(jnp.int32, (heads, 128), 1)
    for s in range(seqs):
        per_head = []
        for h in range(heads):
            found = lax.dot_general(
                query_new[:, h * key_size : (h + 1) * key_size], keys_by_head[s, h],
                (((1,), (1,)), ((), ())), preferred_element_type=f32,
            )
            per_head.append(found[s : s + 1])
        product = weights[s] * (jnp.concatenate(per_head, axis=0) * inv_root)
        den = jnp.sum(product, axis=1, keepdims=True)
        prob = product.astype(bf16)
        for h in range(heads):
            part_src[s, h : h + 1, 0:value_size] = dot(prob, values_by_head[s, h])[h : h + 1]
        stats = jnp.where(lane == 0, maxes[s], jnp.where(lane == 1, den, anchors[s]))
        part_src[s, 0:heads, value_size : value_size + 128] = stats

    c_copies = []
    for b in range(1, count_kv):
        r = b * count_tp
        c_copies.append(
            remote(part_src.at[target(r)[1]], part_rx.at[b], c_send.at[b], c_recv.at[b], device(r))
        )
    for copy in kv_copies:
        copy.wait_recv()
    copies.extend(kv_copies)
    kv_total = kv_src[block].astype(f32)
    for n in range(1, blocks):
        kv_total += kv_rx[n].astype(f32)
    gates_row = small_sum[pl.ds(kv, 1), :]
    inv_own = lax.rsqrt(
        gates_row[:, 2 * heads_total : 2 * heads_total + 1] / model_width + epsilon
    )
    gates_row = gates_row * inv_own
    query_own = q_sum[pl.ds(kv, 1), :]
    kv_row = jnp.concatenate([kv_total[0:1], kv_total[1:2]], axis=1) * inv_own
    kv_row = kv_row.astype(bf16).astype(f32)
    own = []
    for h in range(heads):
        key_h = kv_row[:, h * key_size : (h + 1) * key_size]
        value_h = kv_row[:, width_q + h * value_size : width_q + (h + 1) * value_size]
        query_h = query_own[:, h * key_size : (h + 1) * key_size]
        score = jnp.sum(query_h * key_h, axis=1, keepdims=True) * inv_root
        in_gate = gates_row[:, h : h + 1]
        forget = gates_row[:, heads_total + h : heads_total + h + 1]
        for c in range(1, count_tp):
            at = c * heads + h
            in_gate = jnp.where(tp == c, gates_row[:, at : at + 1], in_gate)
            at = heads_total + at
            forget = jnp.where(tp == c, gates_row[:, at : at + 1], forget)
        log_forget = jnp.minimum(forget, 0.0) - jnp.log1p(jnp.exp(-jnp.abs(forget)))
        own.append((score, score.astype(bf16).astype(f32) * value_h, in_gate, log_forget))
    for copy in c_copies:
        copy.wait_recv()
    copies.extend(c_copies)
    parts = [part_src[kv]] + [part_rx[b] for b in range(1, count_kv)]
    outs = []
    for h in range(heads):
        tops = [p[h : h + 1, value_size : value_size + 1] for p in parts]
        cache_max = functools.reduce(jnp.maximum, tops)
        anchor = functools.reduce(
            jnp.maximum, [p[h : h + 1, value_size + 2 : value_size + 3] for p in parts]
        )
        scale = [jnp.exp(t - cache_max) for t in tops]
        cache_den = sum(z * p[h : h + 1, value_size + 1 : value_size + 2] for z, p in zip(scale, parts))
        cache_num = sum(z * p[h : h + 1, 0:value_size] for z, p in zip(scale, parts))
        score, own_num, in_gate, log_forget = own[h]
        carried = anchor + log_forget + cache_max
        highest = jnp.maximum(carried, in_gate)
        weight_cache = jnp.exp(carried - highest)
        weight_own = jnp.exp(in_gate - highest)
        den = weight_cache * cache_den + weight_own * score
        num = weight_cache * cache_num + weight_own * own_num
        outs.append(num / jnp.maximum(jnp.abs(den), 1.0))
    heads_row = jnp.concatenate(outs, axis=1)
    heads_rx[me] = jnp.concatenate([heads_row[:, :half_v], heads_row[:, half_v:]], axis=0).astype(bf16)
    d_copies = [
        remote(heads_rx.at[me], heads_rx.at[me], d_send.at[r], d_recv.at[r], device(r))
        for r in near[::-1]
    ]
    loaded(wo_v, 6)
    for copy in d_copies:
        copy.wait_recv()
    copies.extend(d_copies)
    for j in range(count):
        row, c = j // count_tp, j % count_tp
        pair = heads_rx[j].astype(f32)
        for i in range(2):
            start = c * width_v + i * half_v
            heads_all[row : row + 1, start : start + half_v] = pair[i : i + 1]
    attended = dot(heads_all[...].astype(bf16), wo_v[...])
    own_cols = tokens[:, pl.ds(pl.multiple_of(tp * out_block, out_block), out_block)].astype(f32)
    residual = (own_cols + attended).astype(bf16)
    resid_rx[me] = residual
    e_copies = {
        r: remote(resid_rx.at[me], resid_rx.at[me], e_send.at[r], e_recv.at[r], device(r))
        for r in near[::-1]
    }
    loaded(wgate_v, 7)
    loaded(wup_v, 8)
    gate_act = up_act = square = 0.0
    order = [0] + near
    for first in range(0, count, 4):
        group = order[first : first + 4]
        for r in group:
            if r:
                e_copies[r].wait_recv()
                copies.append(e_copies[r])
        for r in group:
            at = source(r) if r else me
            piece = resid_rx[at].astype(f32) if r else residual.astype(f32)
            square += jnp.sum(piece * piece, axis=1, keepdims=True)
            piece = (piece * gain_row(1, at, out_block)).astype(bf16)
            span = pl.ds(pl.multiple_of(at * out_block, out_block), out_block)
            gate_act += dot(piece, wgate_v[span, :])
            up_act += dot(piece, wup_v[span, :])
    inv_ffn = lax.rsqrt(square / model_width + epsilon)
    gate_act = gate_act * inv_ffn
    up_act = up_act * inv_ffn
    hidden = (gate_act / (1.0 + jnp.exp(-gate_act)) * up_act).astype(bf16)
    loaded(wdown_v, 9)
    f_copies = []
    order = near[::-1]
    for first in range(0, count - 1, 4):
        group = order[first : first + 4]
        for r in group:
            t = target(r)
            j = (t[0] * count_kv + t[1]) * count_tp + t[2]
            down_src[r] = dot(hidden, wdown_v[j]).astype(bf16)
        for r in group:
            f_copies.append(
                remote(down_src.at[r], down_rx.at[r], f_send.at[r], f_recv.at[r], device(r))
            )
    total = residual.astype(f32) + dot(hidden, wdown_v[me])
    for r, copy in zip(near, f_copies[::-1]):
        copy.wait_recv()
        copies.append(copy)
        total += down_rx[r].astype(f32)
    out_ref[...] = total.astype(bf16)
    for copy in copies:
        copy.wait_send()


def fused(
    tokens, lengths, cache_keys, cache_values, cache_igate, cache_fcum, gain_mix,
    w_query, w_key, w_value, w_gates, w_out, gain_ffn, w_gate, w_up, w_down,
):
    sizes = tuple(lax.axis_size(name) for name in ("dp", "kv", "tp"))
    count = sizes[0] * sizes[1] * sizes[2]
    blocks = sizes[0] * sizes[1]
    f32, bf16 = jnp.float32, jnp.bfloat16
    rows, feat = tokens.shape
    seqs, block_len, heads, key_size = cache_keys.shape
    value_size = cache_values.shape[3]
    out_block = w_out.shape[1]
    half_kv = heads * (key_size + value_size) // 2
    half_v = heads * value_size // 2
    anywhere = pl.BlockSpec(memory_space=pl.ANY)
    vmem = pl.BlockSpec(memory_space=pltpu.VMEM)
    dma = pltpu.SemaphoreType.DMA
    scratch = [
        pltpu.VMEM(w_query.shape, bf16),
        pltpu.VMEM(w_key.shape, bf16),
        pltpu.VMEM(w_value.shape, bf16),
        pltpu.VMEM((w_gates.shape[1], feat), bf16),
        pltpu.VMEM(w_out.shape, bf16),
        pltpu.VMEM(w_gate.shape, bf16),
        pltpu.VMEM(w_up.shape, bf16),
        pltpu.VMEM((count, w_down.shape[0], out_block), bf16),
        pltpu.VMEM((seqs, heads, block_len, key_size), bf16),
        pltpu.VMEM((seqs, heads, block_len, value_size), bf16),
        pltpu.VMEM((sizes[0], seqs, heads * key_size), bf16),
        pltpu.VMEM((rows, 2, half_kv), bf16),
        pltpu.VMEM((sizes[0], seqs, 128), f32),
        pltpu.VMEM((blocks, seqs, heads * key_size), bf16),
        pltpu.VMEM((blocks, 2, half_kv), bf16),
        pltpu.VMEM((blocks, seqs, 128), f32),
        pltpu.VMEM((seqs, 128), f32),
        pltpu.VMEM((seqs, heads * key_size), f32),
        pltpu.VMEM((seqs, 4, value_size + 128), f32),
        pltpu.VMEM((sizes[1], 4, value_size + 128), f32),
        pltpu.VMEM((count, 2, half_v), bf16),
        pltpu.VMEM((rows, w_out.shape[0]), f32),
        pltpu.VMEM((count, rows, out_block), bf16),
        pltpu.VMEM((count, rows, out_block), bf16),
        pltpu.VMEM((count, rows, out_block), bf16),
        pltpu.VMEM((2, blocks * feat // 128, 128), f32),
        dma((10,)),
        dma((3, blocks)), dma((3, blocks)),
        dma((sizes[1],)), dma((sizes[1],)),
        dma((count,)), dma((count,)),
        dma((count,)), dma((count,)),
        dma((count,)), dma((count,)),
    ]
    return pl.pallas_call(
        functools.partial(fused_kernel, sizes),
        out_shape=jax.ShapeDtypeStruct((rows, out_block), bf16),
        in_specs=[pl.BlockSpec(memory_space=pltpu.SMEM)] + [vmem] * 5 + [anywhere] * 10,
        out_specs=vmem,
        scratch_shapes=scratch,
        compiler_params=pltpu.CompilerParams(
            collective_id=0, has_side_effects=True, vmem_limit_bytes=60 * 1024 * 1024
        ),
    )(
        lengths, tokens, cache_igate.swapaxes(0, 1), cache_fcum.swapaxes(0, 1),
        gain_mix.reshape(-1, 128), gain_ffn.reshape(-1, 128),
        cache_keys.swapaxes(1, 2), cache_values.swapaxes(1, 2),
        w_query, w_key, w_value, w_gates.T, w_out, w_gate, w_up, w_down,
    )


def fits_kernel(tokens, cache_keys, w_out, w_gate):
    return (
        cache_keys.shape[0] == lax.axis_size("kv")
        and cache_keys.shape[2] <= 4
        and tokens.shape[1] % 128 == 0
        and w_out.shape[1] % 128 == 0
        and w_gate.shape[1] % 128 == 0
    )


def layer(*args):
    if fits_kernel(args[0], args[2], args[11], args[13]):
        return fused(*args)
    return per_device(*args)


def solution(mesh):
    in_specs = (
        P("grp", ("dp", "kv")),
        P(("grp", "dp")),
        P(("grp", "dp"), "kv", "tp", None),
        P(("grp", "dp"), "kv", "tp", None),
        P(("grp", "dp"), "tp", "kv"),
        P(("grp", "dp"), "tp", "kv"),
        P(),
        P(("dp", "kv"), "tp"),
        P(("dp", "kv"), "tp"),
        P(("dp", "kv"), "tp"),
        P(),
        P(None, ("dp", "kv", "tp")),
        P(),
        P(None, ("dp", "kv", "tp")),
        P(None, ("dp", "kv", "tp")),
        P(("dp", "kv", "tp"), None),
    )
    out_specs = P("grp", ("dp", "kv", "tp"))
    return jax.shard_map(
        layer, mesh=mesh, in_specs=in_specs, out_specs=out_specs, check_vma=False
    )
```

profile of v0, /device:TPU:0, one launch (start us, length us, event | category | flops | bytes accessed | tf_op | source)
XLA Modules:
  0.0 34.5 jit_solution(12775991980674603341)
XLA Ops:
  0.0 33.3 %shard_map.154 = bf16[8,256]{1,0:T(8,128)(2,1)} custom-call(s32[4]{0:T(128)} %lengths.1, bf16[8,512]{1,0:T(8,128)(2,1)} %tokens.1, f32[3,4,128]{2,1,0:T(4,128)} %bitcast.12, f32[3,4,128]{2,1,0:T(4,128)} %bitcast.13, bf16[32,128]{1,0:T(8,128)(2,1)} %bitcast.10, bf16[32,128]{1,0:T(8,128)(2,1)} %bitcast.11, bf16[4,3,128,256]{3,2,1,0:T(8,128)(2,1)} %bitcast.8, ...), custom_call_target="tpu_custom_call" | custom-call | tf_op jit(solution)/shard_map/pallas_call | solution.py:537
  33.3 1.3 %copy.18 = bf16[8,256]{1,0:T(8,128)(2,1)} copy(bf16[8,256]{1,0:T(8,128)(2,1)} %shard_map.154) | data formatting | bytes 8192
where the time goes:
time: 34.8 us; the launch traced here: 34.5 us
  Pallas kernels  33.3 us (96%)
  local copies, waits for them, and re-layouts  1.28 us (4%)
    pallas_call x1, Pallas kernels, fused(): pl.pallas_call(functools.partial(fused_kernel, sizes), out_shape=jax.Shap...  33.3 us
    unnamed x1, local copies, waits for them, and re-layouts  1.28 us

commit v1 on v0

v1 whole, which is shorter than its diff:
```python
import functools

import jax
import jax.numpy as jnp
from jax import lax
from jax.experimental import pallas as pl
from jax.experimental.pallas import tpu as pltpu
from jax.sharding import PartitionSpec as P

epsilon = 1e-06
very_low = -1e30


def combined_all(value, axis, join):
    pieces = jax.tree.map(lambda part: lax.all_gather(part, axis), value)
    head = jax.tree.map(lambda part: part[0], pieces)
    tail = jax.tree.map(lambda part: part[1:], pieces)
    total, _ = lax.scan(lambda total, piece: (join(total, piece), None), head, tail)
    return total


def merge_partial(first_part, second_part):
    max_first, den_first, num_first, anchor_first = first_part
    max_second, den_second, num_second, anchor_second = second_part
    highest = jnp.maximum(max_first, max_second)
    scale_first = jnp.exp(max_first - highest)
    scale_second = jnp.exp(max_second - highest)
    denominator = scale_first * den_first + scale_second * den_second
    numerator = scale_first[..., None] * num_first + scale_second[..., None] * num_second
    return (highest, denominator, numerator, jnp.maximum(anchor_first, anchor_second))


def per_device(
    tokens,
    lengths,
    cache_keys,
    cache_values,
    cache_igate,
    cache_fcum,
    gain_mix,
    w_query,
    w_key,
    w_value,
    w_gates,
    w_out,
    gain_ffn,
    w_gate,
    w_up,
    w_down,
):
    count_dp = lax.axis_size("dp")
    count_kv = lax.axis_size("kv")
    count_tp = lax.axis_size("tp")
    index_dp = lax.axis_index("dp")
    index_kv = lax.axis_index("kv")
    index_tp = lax.axis_index("tp")
    row_count, feat_block = tokens.shape
    seq_count, block_len, head_local, key_dimension = cache_keys.shape
    value_size = cache_values.shape[3]
    model_width = gain_mix.shape[0]
    heads_total = w_gates.shape[1] // 2
    out_block = w_out.shape[1]
    col_start = (index_dp * count_kv + index_kv) * feat_block
    token_f32 = tokens.astype(jnp.float32)
    gain_part = lax.dynamic_slice_in_dim(gain_mix, col_start, feat_block, 0).astype(jnp.float32)
    scaled = (token_f32 * gain_part[None, :]).astype(jnp.bfloat16)
    energy = jnp.sum(token_f32 * token_f32, axis=1)
    joined = jnp.concatenate(
        [
            jnp.dot(scaled, w_query, preferred_element_type=jnp.float32),
            jnp.dot(scaled, w_key, preferred_element_type=jnp.float32),
            jnp.dot(scaled, w_value, preferred_element_type=jnp.float32),
        ],
        axis=1,
    )
    gate_rows = lax.dynamic_slice_in_dim(w_gates, col_start, feat_block, 0).reshape(
        feat_block, 2, heads_total
    )
    gate_cols = lax.dynamic_slice_in_dim(gate_rows, index_tp * head_local, head_local, 2).reshape(
        feat_block, 2 * head_local
    )
    gate_part = jnp.dot(scaled, gate_cols, preferred_element_type=jnp.float32)
    joined_part, gate_rowsum, energy_part = (
        lax.psum_scatter(joined, "dp", scatter_dimension=0, tiled=True),
        lax.psum_scatter(gate_part, "dp", scatter_dimension=0, tiled=True),
        lax.psum_scatter(energy, "dp", scatter_dimension=0, tiled=True),
    )
    joined_own, gate_own, energy_own = lax.psum((joined_part, gate_rowsum, energy_part), "kv")
    inv_norm = lax.rsqrt(energy_own / model_width + epsilon)[:, None]
    width_qk = head_local * key_dimension
    query_new = (
        (joined_own[:, :width_qk] * inv_norm)
        .astype(jnp.bfloat16)
        .reshape(seq_count, head_local, key_dimension)
    )
    new_key = (
        (joined_own[:, width_qk : 2 * width_qk] * inv_norm)
        .astype(jnp.bfloat16)
        .reshape(seq_count, head_local, key_dimension)
    )
    new_value = (
        (joined_own[:, 2 * width_qk :] * inv_norm)
        .astype(jnp.bfloat16)
        .reshape(seq_count, head_local, value_size)
    )
    gates_now = gate_own * inv_norm
    in_gate = gates_now[:, :head_local]
    log_forget = jax.nn.log_sigmoid(gates_now[:, head_local:])
    inv_root = key_dimension ** (-0.5)
    scores = (
        jnp.einsum("shk,sphk->shp", query_new, cache_keys, preferred_element_type=jnp.float32)
        * inv_root
    )
    positions = index_kv * block_len + jnp.arange(block_len, dtype=jnp.int32)
    is_live = positions[None, None, :] < lengths[:, None, None]
    exponent = jnp.where(is_live, cache_igate - cache_fcum, very_low)
    block_max = jnp.max(exponent, axis=2)
    weight = jnp.where(is_live, jnp.exp(exponent - block_max[..., None]), 0.0)
    product = weight * scores
    block_den = jnp.sum(product, axis=2)
    block_num = jnp.einsum(
        "shp,sphv->shv",
        product.astype(jnp.bfloat16),
        cache_values,
        preferred_element_type=jnp.float32,
    )
    holding = positions[None, None, :] == (lengths - 1)[:, None, None]
    anchor = jnp.max(jnp.where(holding, cache_fcum, very_low), axis=2)
    cache_max, cache_den, cache_num, anchor_all = combined_all(
        (block_max, block_den, block_num, anchor), "kv", merge_partial
    )
    own_score = (
        jnp.sum(query_new.astype(jnp.float32) * new_key.astype(jnp.float32), axis=2) * inv_root
    )
    own_prob = lax.optimization_barrier(own_score.astype(jnp.bfloat16)).astype(jnp.float32)
    own_num = own_prob[..., None] * new_value.astype(jnp.float32)
    carried = anchor_all + log_forget
    highest = jnp.maximum(carried + cache_max, in_gate)
    weight_cache = jnp.exp(carried + cache_max - highest)
    weight_own = jnp.exp(in_gate - highest)
    denominator = weight_cache * cache_den + weight_own * own_score
    numerator = weight_cache[..., None] * cache_num + weight_own[..., None] * own_num
    heads_out = (numerator / jnp.maximum(jnp.abs(denominator), 1.0)[..., None]).astype(jnp.bfloat16)
    heads_out = heads_out.reshape(seq_count, head_local * value_size)
    gathered = lax.all_gather(heads_out[None], ("dp", "tp"), axis=0, tiled=True)
    gathered = gathered.reshape(count_dp, count_tp, seq_count, head_local * value_size)
    out_weight = w_out.reshape(count_tp, head_local * value_size, out_block)
    attended = jnp.einsum(
        "atsk,tkc->asc", gathered, out_weight, preferred_element_type=jnp.float32
    ).reshape(row_count, out_block)
    own_cols = lax.dynamic_slice_in_dim(token_f32, index_tp * out_block, out_block, 1)
    residual = (own_cols + attended).astype(jnp.bfloat16)
    full_rows = lax.all_gather(residual, ("dp", "kv", "tp"), axis=1, tiled=True)
    full_f32 = full_rows.astype(jnp.float32)
    inv_norm_ffn = lax.rsqrt(jnp.mean(full_f32 * full_f32, axis=1, keepdims=True) + epsilon)
    normed = (full_f32 * inv_norm_ffn * gain_ffn.astype(jnp.float32)[None, :]).astype(jnp.bfloat16)
    gate_act = jnp.dot(normed, w_gate, preferred_element_type=jnp.float32)
    up_act = jnp.dot(normed, w_up, preferred_element_type=jnp.float32)
    hidden = (jax.nn.silu(gate_act) * up_act).astype(jnp.bfloat16)
    summed = lax.psum_scatter(
        lax.dot_general(
            w_down, hidden, (((0,), (1,)), ((), ())), preferred_element_type=jnp.float32
        ),
        ("dp", "kv", "tp"),
        scatter_dimension=0,
        tiled=True,
    )
    return (residual.astype(jnp.float32) + summed.T).astype(jnp.bfloat16)


def fused_kernel(
    sizes, lengths, tokens, cache_igate, cache_fcum, gain_mix, gain_ffn,
    cache_keys, cache_values, w_query, w_key, w_value, w_gates, w_out, w_gate, w_up, w_down,
    out_ref,
    len_s, tok_v, igate_v, fcum_v, gain_raw,
    wq_v, wk_v, wv_v, wg_v, wo_v, wgate_v, wup_v, wdown_v,
    keys_v, values_v,
    q_src, kv_src, small_src, q_rx, kv_rx, small_rx,
    part_src, part_rx, heads_rx, resid_rx, down_src, down_rx, gains,
    load_sem, send_sem, recv_sem,
):
    count_dp, count_kv, count_tp = sizes
    count = count_dp * count_kv * count_tp
    blocks = count_dp * count_kv
    dp, kv, tp = lax.axis_index("dp"), lax.axis_index("kv"), lax.axis_index("tp")
    f32, bf16 = jnp.float32, jnp.bfloat16
    seqs, heads, block_len, key_size = cache_keys.shape
    value_size = cache_values.shape[3]
    rows, feat = tokens.shape
    width_q = heads * key_size
    width_v = heads * value_size
    half_kv = (width_q + width_v) // 2
    out_block = out_ref.shape[1]
    model_width = feat * blocks
    heads_total = heads * count_tp
    block = dp * count_kv + kv
    me = block * count_tp + tp

    def split(r):
        return r // (count_kv * count_tp), (r // count_tp) % count_kv, r % count_tp

    def target(r):
        a, b, c = split(r)
        return dp ^ a, kv ^ b, tp ^ c

    def place(r):
        t = target(r)
        return (t[0] * count_kv + t[1]) * count_tp + t[2]

    def device(r):
        t = target(r)
        return {"dp": t[0], "kv": t[1], "tp": t[2]}

    def distance(r):
        a, b, c = split(r)
        return (a + b) * 2 + c

    near = sorted(range(1, count), key=distance)
    peers = sorted(range(count_tp, count, count_tp), key=distance)[::-1]

    def gain_row(which, at, width):
        lines = width // 128
        first = at * lines
        return jnp.concatenate(
            [gains[which, pl.ds(first + i, 1), :] for i in range(lines)], axis=1
        )

    def load(hbm, vmem, index, pieces=1):
        step = hbm.shape[0] // pieces
        for i in range(pieces):
            pltpu.make_async_copy(
                hbm.at[pl.ds(i * step, step)], vmem.at[pl.ds(i * step, step)], load_sem.at[index]
            ).start()

    def loaded(vmem, index):
        pltpu.make_async_copy(vmem, vmem, load_sem.at[index]).wait()

    def remote(src, dst, send, recv, r):
        pltpu.make_async_remote_copy(
            src_ref=src, dst_ref=dst, send_sem=send_sem.at[send], recv_sem=recv_sem.at[recv],
            device_id=device(r), device_id_type=pl.DeviceIdType.MESH,
        ).start()

    def arrived(like, recv):
        pltpu.make_async_copy(like, like, recv_sem.at[recv]).wait()

    def sent(like, send):
        pltpu.make_async_copy(like, like, send_sem.at[send]).wait()

    barrier = pltpu.get_barrier_semaphore()
    for r in near[::-1]:
        pl.semaphore_signal(
            barrier, inc=1, device_id=device(r), device_id_type=pl.DeviceIdType.MESH
        )
    load(tokens, tok_v, 0)
    load(gain_mix, gain_raw.at[0], 1)
    gate_start = pl.multiple_of(block * feat, feat)
    pltpu.make_async_copy(w_gates.at[:, pl.ds(gate_start, feat)], wg_v, load_sem.at[3]).start()
    load(w_query, wq_v, 4, 4)
    load(lengths, len_s, 2)
    load(cache_igate, igate_v, 5)
    load(cache_fcum, fcum_v, 6)
    load(w_key, wk_v, 7, 2)
    load(w_value, wv_v, 8, 4)

    dot = functools.partial(jnp.dot, preferred_element_type=f32)
    loaded(tok_v, 0)
    loaded(gain_raw.at[0], 1)
    gains[0] = gain_raw[0].astype(f32)
    token = tok_v[...].astype(f32)
    scaled = (token * gain_row(0, block, feat)).astype(bf16)
    energy = jnp.sum(token * token, axis=1, keepdims=True)
    loaded(wg_v, 3)
    gate_part = lax.dot_general(
        scaled, wg_v[...], (((1,), (1,)), ((), ())), preferred_element_type=f32
    )
    gate_part = jnp.concatenate(
        [gate_part, jnp.zeros((rows, 128 - 2 * heads_total), f32)], axis=1
    )
    shifted = gate_part
    for c in range(1, count_tp):
        shifted = jnp.where(tp == c, pltpu.roll(gate_part, 128 - c * heads, 1), shifted)
    lane_all = lax.broadcasted_iota(jnp.int32, (rows, 128), 1)
    at_energy, at_max, at_anchor = 16, 32, 64
    shifted = jnp.where(lane_all == at_energy, energy, shifted)

    loaded(len_s, 2)
    loaded(igate_v, 5)
    loaded(fcum_v, 6)
    lane = lax.broadcasted_iota(jnp.int32, (seqs, 128), 1)
    row = lax.broadcasted_iota(jnp.int32, (seqs, block_len), 0)
    row_v = lax.broadcasted_iota(jnp.int32, (seqs, value_size), 0)
    length = jnp.zeros((seqs, block_len), jnp.int32)
    for s in range(seqs):
        length = jnp.where(row == s, len_s[s], length)
    position = kv * block_len + lax.broadcasted_iota(jnp.int32, (seqs, block_len), 1)
    live = position < length
    holding = position == length - 1
    exponents = []
    stats = jnp.full((seqs, 128), very_low, f32)
    for h in range(heads):
        fcum = fcum_v[h]
        exponent = jnp.where(live, igate_v[h] - fcum, very_low)
        exponents.append(exponent)
        top = jnp.max(exponent, axis=1, keepdims=True)
        anchor = jnp.max(jnp.where(holding, fcum, very_low), axis=1, keepdims=True)
        stats = jnp.where(lane == at_max + h, top, stats)
        stats = jnp.where(lane == at_anchor + h, anchor, stats)
    for a in range(count_dp):
        part = shifted[a * seqs : (a + 1) * seqs]
        small_src[a] = jnp.where(lane < at_max, part, stats)

    loaded(wq_v, 4)
    query = dot(scaled, wq_v[...])
    for a in range(count_dp):
        q_src[a] = query[a * seqs : (a + 1) * seqs].astype(bf16)
    pl.semaphore_wait(barrier, count - 1)
    for r in peers:
        n, to = r // count_tp, target(r)[0]
        remote(small_src.at[to], small_rx.at[n], 0, 0, r)
        remote(q_src.at[to], q_rx.at[n], 1, 1, r)
    for s in range(seqs):
        span = pl.ds(s * block_len, block_len)
        pltpu.make_async_copy(cache_keys.at[s], keys_v.at[:, span, :], load_sem.at[9]).start()
    for s in range(seqs):
        span = pl.ds(s * block_len, block_len)
        pltpu.make_async_copy(cache_values.at[s], values_v.at[:, span, :], load_sem.at[10]).start()
    loaded(wk_v, 7)
    key_part = dot(scaled, wk_v[...])
    loaded(wv_v, 8)
    load(w_out, wo_v, 11, 4)
    load(gain_ffn, gain_raw.at[1], 15)
    load(w_gate, wgate_v, 12, 8)
    load(w_up, wup_v, 13, 8)
    for j in range(count):
        pltpu.make_async_copy(
            w_down.at[:, pl.ds(j * out_block, out_block)], wdown_v.at[j], load_sem.at[14]
        ).start()
    value_part = dot(scaled, wv_v[...])
    joined = jnp.concatenate([key_part, value_part], axis=1)
    for i in range(rows):
        line = joined[i : i + 1]
        kv_src[i] = jnp.concatenate([line[:, :half_kv], line[:, half_kv:]], axis=0).astype(bf16)
    for r in peers:
        t = target(r)
        remote(kv_src.at[t[0] * count_kv + t[1]], kv_rx.at[r // count_tp], 2, 2, r)

    arrived(small_rx.at[pl.ds(1, blocks - 1)], 0)
    small = small_src[dp]
    extreme = small
    for n in range(1, blocks):
        small += small_rx[n]
        if n < count_kv:
            extreme = jnp.maximum(extreme, small_rx[n])
    inv_norm = lax.rsqrt(small[:, at_energy : at_energy + 1] / model_width + epsilon)
    gates_now = small * inv_norm
    log_forget = jnp.minimum(gates_now, 0.0) - jnp.log1p(jnp.exp(-jnp.abs(gates_now)))
    forget_here = pltpu.roll(log_forget, 128 - heads_total, 1)
    top_here = pltpu.roll(extreme, 128 - at_max, 1)
    carried = pltpu.roll(extreme, 128 - at_anchor, 1) + forget_here
    highest = jnp.maximum(carried + top_here, gates_now)
    offset = carried - highest
    own_weight = jnp.exp(gates_now - highest)
    weights = []
    for h in range(heads):
        power = jnp.where(live, exponents[h] + offset[:, h : h + 1], very_low)
        weights.append(jnp.where(live, jnp.exp(power), 0.0))

    arrived(q_rx.at[pl.ds(1, blocks - 1)], 1)
    q_total = q_src[dp].astype(f32)
    for n in range(1, blocks):
        q_total += q_rx[n].astype(f32)
    query_new = (q_total * inv_norm).astype(bf16)
    loaded(keys_v, 9)
    inv_root = key_size ** (-0.5)
    probs, dens, nums = [], [], []
    for h in range(heads):
        found = lax.dot_general(
            query_new[:, h * key_size : (h + 1) * key_size], keys_v[h],
            (((1,), (1,)), ((), ())), preferred_element_type=f32,
        )
        score = found[:, 0:block_len]
        for s in range(1, seqs):
            score = jnp.where(row == s, found[:, s * block_len : (s + 1) * block_len], score)
        product = weights[h] * (score * inv_root)
        dens.append(jnp.sum(product, axis=1, keepdims=True))
        probs.append(
            jnp.concatenate([jnp.where(row == s, product, 0.0) for s in range(seqs)], axis=1).astype(bf16)
        )
    loaded(values_v, 10)
    for h in range(heads):
        nums.append(dot(probs[h], values_v[h]))

    arrived(kv_rx.at[pl.ds(1, blocks - 1)], 2)
    kv_total = kv_src[block].astype(f32)
    for n in range(1, blocks):
        kv_total += kv_rx[n].astype(f32)
    kv_row = jnp.concatenate([kv_total[0:1], kv_total[1:2]], axis=1)
    kv_row = (jnp.broadcast_to(kv_row, (seqs, 2 * half_kv)) * inv_norm).astype(bf16).astype(f32)
    query_f32 = query_new.astype(f32)
    mine = lax.broadcasted_iota(jnp.int32, (seqs, 1), 0) == kv
    den_line = jnp.zeros((seqs, 128), f32)
    for h in range(heads):
        key_h = kv_row[:, h * key_size : (h + 1) * key_size]
        value_h = kv_row[:, width_q + h * value_size : width_q + (h + 1) * value_size]
        query_h = query_f32[:, h * key_size : (h + 1) * key_size]
        score = jnp.sum(query_h * key_h, axis=1, keepdims=True) * inv_root
        own = jnp.where(mine, own_weight[:, h : h + 1], 0.0)
        dens[h] += own * score
        nums[h] += (own * score.astype(bf16).astype(f32)) * value_h
        coarse = dens[h].astype(bf16).astype(f32)
        den_line = jnp.where(lane == h, coarse, den_line)
        den_line = jnp.where(lane == heads + h, dens[h] - coarse, den_line)
        part_src[:, h * value_size : (h + 1) * value_size] = nums[h].astype(bf16)
    part_src[:, width_v : width_v + 128] = den_line.astype(bf16)
    for b in range(count_kv - 1, 0, -1):
        remote(part_src, part_rx.at[b], 3, 3, b * count_tp)

    if count_kv > 1:
        arrived(part_rx.at[pl.ds(1, count_kv - 1)], 3)
    tail = part_rx[1, :, width_v : width_v + 128].astype(f32)
    for b in range(2, count_kv):
        tail += part_rx[b, :, width_v : width_v + 128].astype(f32)
    for h in range(heads):
        span = pl.ds(h * value_size, value_size)
        num = nums[h]
        for b in range(1, count_kv):
            num += part_rx[b, :, span].astype(f32)
        den = dens[h] + tail[:, h : h + 1] + tail[:, heads + h : heads + h + 1]
        heads_rx[dp * count_tp + tp, :, span] = (num / jnp.maximum(jnp.abs(den), 1.0)).astype(bf16)
    d_peers = [r for r in near[::-1] if split(r)[1] == 0]
    for r in d_peers:
        remote(heads_rx.at[dp * count_tp + tp], heads_rx.at[dp * count_tp + tp], 4, 4, r)
    loaded(wo_v, 11)
    loaded(gain_raw.at[1], 15)
    gains[1] = gain_raw[1].astype(f32)
    arrived(heads_rx.at[pl.ds(0, len(d_peers))], 4)
    lines = [
        jnp.concatenate([heads_rx[a * count_tp + c].astype(f32) for c in range(count_tp)], axis=1)
        for a in range(count_dp)
    ]
    attended = dot(jnp.concatenate(lines, axis=0).astype(bf16), wo_v[...])
    own_cols = tok_v[:, pl.ds(pl.multiple_of(tp * out_block, out_block), out_block)].astype(f32)
    residual = (own_cols + attended).astype(bf16)
    resid_rx[me] = residual
    levels = sorted({distance(r) // 2 for r in range(count)})
    groups = [[r for r in [0] + near if distance(r) // 2 == level] for level in levels]
    which = {r: i for i, group in enumerate(groups) for r in group}
    for r in near[::-1]:
        remote(resid_rx.at[me], resid_rx.at[me], 5, 5 + which[r], r)
    loaded(wgate_v, 12)
    loaded(wup_v, 13)
    gate_act = up_act = square = 0.0
    for i, group in enumerate(groups):
        others = sum(r > 0 for r in group)
        arrived(resid_rx.at[pl.ds(0, others)], 5 + i)
        for r in group:
            at = place(r)
            piece = resid_rx[at].astype(f32) if r else residual.astype(f32)
            square += jnp.sum(piece * piece, axis=1, keepdims=True)
            piece = (piece * gain_row(1, at, out_block)).astype(bf16)
            span = pl.ds(pl.multiple_of(at * out_block, out_block), out_block)
            gate_act += dot(piece, wgate_v[span, :])
            up_act += dot(piece, wup_v[span, :])
    inv_ffn = lax.rsqrt(square / model_width + epsilon)
    gate_act = gate_act * inv_ffn
    up_act = up_act * inv_ffn
    hidden = (gate_act / (1.0 + jnp.exp(-gate_act)) * up_act).astype(bf16)
    loaded(wdown_v, 14)
    last = 5 + len(groups)
    order = near[::-1]
    for first in range(0, count - 1, 2):
        pair = order[first : first + 2]
        for r in pair:
            down_src[r] = dot(hidden, wdown_v[place(r)]).astype(bf16)
        for r in pair:
            remote(down_src.at[r], down_rx.at[r], 6, last, r)
    total = residual.astype(f32) + dot(hidden, wdown_v[me])
    sent(small_rx.at[pl.ds(1, blocks - 1)], 0)
    sent(q_rx.at[pl.ds(1, blocks - 1)], 1)
    sent(kv_rx.at[pl.ds(1, blocks - 1)], 2)
    if count_kv > 1:
        sent(part_rx.at[pl.ds(1, count_kv - 1)], 3)
    sent(heads_rx.at[pl.ds(0, len(d_peers))], 4)
    sent(resid_rx.at[pl.ds(0, count - 1)], 5)
    arrived(down_rx.at[pl.ds(1, count - 1)], last)
    for r in near:
        total += down_rx[r].astype(f32)
    out_ref[...] = total.astype(bf16)
    sent(down_rx.at[pl.ds(1, count - 1)], 6)


def fused(
    tokens, lengths, cache_keys, cache_values, cache_igate, cache_fcum, gain_mix,
    w_query, w_key, w_value, w_gates, w_out, gain_ffn, w_gate, w_up, w_down,
):
    sizes = tuple(lax.axis_size(name) for name in ("dp", "kv", "tp"))
    count = sizes[0] * sizes[1] * sizes[2]
    blocks = sizes[0] * sizes[1]
    f32, bf16 = jnp.float32, jnp.bfloat16
    rows, feat = tokens.shape
    seqs, block_len, heads, key_size = cache_keys.shape
    value_size = cache_values.shape[3]
    out_block = w_out.shape[1]
    half_kv = heads * (key_size + value_size) // 2
    width_v = heads * value_size
    hbm = pl.BlockSpec(memory_space=pl.ANY)
    vmem = pl.BlockSpec(memory_space=pltpu.VMEM)
    dma = pltpu.SemaphoreType.DMA
    scratch = [
        pltpu.SMEM((seqs,), jnp.int32),
        pltpu.VMEM(tokens.shape, bf16),
        pltpu.VMEM((heads, seqs, block_len), f32),
        pltpu.VMEM((heads, seqs, block_len), f32),
        pltpu.VMEM((2, blocks * feat // 128, 128), bf16),
        pltpu.VMEM(w_query.shape, bf16),
        pltpu.VMEM(w_key.shape, bf16),
        pltpu.VMEM(w_value.shape, bf16),
        pltpu.VMEM((w_gates.shape[1], feat), bf16),
        pltpu.VMEM(w_out.shape, bf16),
        pltpu.VMEM(w_gate.shape, bf16),
        pltpu.VMEM(w_up.shape, bf16),
        pltpu.VMEM((count, w_down.shape[0], out_block), bf16),
        pltpu.VMEM((heads, seqs * block_len, key_size), bf16),
        pltpu.VMEM((heads, seqs * block_len, value_size), bf16),
        pltpu.VMEM((sizes[0], seqs, heads * key_size), bf16),
        pltpu.VMEM((rows, 2, half_kv), bf16),
        pltpu.VMEM((sizes[0], seqs, 128), f32),
        pltpu.VMEM((blocks, seqs, heads * key_size), bf16),
        pltpu.VMEM((blocks, 2, half_kv), bf16),
        pltpu.VMEM((blocks, seqs, 128), f32),
        pltpu.VMEM((seqs, width_v + 128), bf16),
        pltpu.VMEM((sizes[1], seqs, width_v + 128), bf16),
        pltpu.VMEM((sizes[0] * sizes[2], seqs, width_v), bf16),
        pltpu.VMEM((count, rows, out_block), bf16),
        pltpu.VMEM((count, rows, out_block), bf16),
        pltpu.VMEM((count, rows, out_block), bf16),
        pltpu.VMEM((2, blocks * feat // 128, 128), f32),
        dma((16,)),
        dma((7,)),
        dma((6 + 5,)),
    ]
    operands = (
        lengths, tokens, cache_igate.swapaxes(0, 1), cache_fcum.swapaxes(0, 1),
        gain_mix.reshape(-1, 128), gain_ffn.reshape(-1, 128),
        cache_keys.swapaxes(1, 2), cache_values.swapaxes(1, 2),
        w_query, w_key, w_value, w_gates.T, w_out, w_gate, w_up, w_down,
    )
    return pl.pallas_call(
        functools.partial(fused_kernel, sizes),
        out_shape=pltpu.VMEM((rows, out_block), bf16),
        in_specs=[hbm] * len(operands),
        out_specs=vmem,
        scratch_shapes=scratch,
        compiler_params=pltpu.CompilerParams(
            collective_id=0, has_side_effects=True, vmem_limit_bytes=40 * 1024 * 1024
        ),
    )(*[pltpu.with_memory_space_constraint(x, pltpu.HBM) for x in operands])


def fits_kernel(tokens, cache_keys, w_out, w_gate):
    return (
        cache_keys.shape[0] == lax.axis_size("kv")
        and all(n in (2, 4) for n in map(lax.axis_size, ("dp", "kv", "tp")))
        and cache_keys.shape[2] <= 4
        and tokens.shape[1] % 128 == 0
        and w_out.shape[1] % 128 == 0
        and w_gate.shape[1] % 128 == 0
    )


def layer(*args):
    if fits_kernel(args[0], args[2], args[11], args[13]):
        return fused(*args)
    return per_device(*args)


def solution(mesh):
    in_specs = (
        P("grp", ("dp", "kv")),
        P(("grp", "dp")),
        P(("grp", "dp"), "kv", "tp", None),
        P(("grp", "dp"), "kv", "tp", None),
        P(("grp", "dp"), "tp", "kv"),
        P(("grp", "dp"), "tp", "kv"),
        P(),
        P(("dp", "kv"), "tp"),
        P(("dp", "kv"), "tp"),
        P(("dp", "kv"), "tp"),
        P(),
        P(None, ("dp", "kv", "tp")),
        P(),
        P(None, ("dp", "kv", "tp")),
        P(None, ("dp", "kv", "tp")),
        P(("dp", "kv", "tp"), None),
    )
    out_specs = P("grp", ("dp", "kv", "tp"))
    return jax.shard_map(
        layer, mesh=mesh, in_specs=in_specs, out_specs=out_specs, check_vma=False
    )
```

time: 34.8 us -> 27.9 us (0.80)
  Pallas kernels: 33.3 us -> 27.1 us
  local copies, waits for them, and re-layouts: 1.28 us -> 0.6 us
    pallas_call x1, Pallas kernels: 33.3 us -> 27.1 us  [fused(): pl.pallas_call(functools.partial(fused_kernel, sizes), out_shape=pltpu.VM...]
    unnamed x1, local copies, waits for them, and re-layouts: 1.28 us -> 0.6 us
where the time goes in v1:
time: 27.9 us; the launch traced here: 27.7 us
  Pallas kernels  27.1 us (97%)
  local copies, waits for them, and re-layouts  0.6 us (2%)
    pallas_call x1, Pallas kernels, fused(): pl.pallas_call(functools.partial(fused_kernel, sizes), out_shape=pltpu.VM...  27.1 us
    unnamed x1, local copies, waits for them, and re-layouts  0.6 us

profile of v1, /device:TPU:0, one launch (start us, length us, event | category | flops | bytes accessed | tf_op | source)
XLA Modules:
  0.0 27.7 jit_solution(2428456875806716234)
XLA Ops:
  0.0 27.1 %shard_map.154 = bf16[8,256]{1,0:T(8,128)(2,1)S(1)} custom-call(s32[4]{0:T(128)} %lengths.1, bf16[8,512]{1,0:T(8,128)(2,1)} %tokens.1, f32[3,4,128]{2,1,0:T(4,128)} %bitcast.12, f32[3,4,128]{2,1,0:T(4,128)} %bitcast.13, bf16[32,128]{1,0:T(8,128)(2,1)} %bitcast.10, bf16[32,128]{1,0:T(8,128)(2,1)} %bitcast.11, bf16[4,3,128,256]{3,2,1,0:T(8,128)(2,1)} %bitcast.8, ...), custom_call_target="tpu_custom_call" | custom-call | tf_op jit(solution)/shard_map/pallas_call | solution.py:549
  27.1 0.6 %copy.18 = bf16[8,256]{1,0:T(8,128)(2,1)} copy(bf16[8,256]{1,0:T(8,128)(2,1)S(1)} %shard_map.154) | data formatting | bytes 8192

commit v2 on v1

--- a/solution.py
+++ b/solution.py
@@ -175,8 +175,8 @@
     len_s, tok_v, igate_v, fcum_v, gain_raw,
     wq_v, wk_v, wv_v, wg_v, wo_v, wgate_v, wup_v, wdown_v,
     keys_v, values_v,
-    q_src, kv_src, small_src, q_rx, kv_rx, small_rx,
-    part_src, part_rx, heads_rx, resid_rx, down_src, down_rx, gains,
+    keys_t, q_src, kv_src, small_src, q_rx, kv_rx, small_rx,
+    own_part, part_src, part_rx, heads_rx, resid_rx, down_src, down_rx, gains,
     load_sem, send_sem, recv_sem,
 ):
     count_dp, count_kv, count_tp = sizes
@@ -195,6 +195,8 @@
     heads_total = heads * count_tp
     block = dp * count_kv + kv
     me = block * count_tp + tp
+    lead = count_tp - 1
+    leads, follows = tp == lead, tp != lead
 
     def split(r):
         return r // (count_kv * count_tp), (r // count_tp) % count_kv, r % count_tp
@@ -216,6 +218,9 @@
         return (a + b) * 2 + c
 
     near = sorted(range(1, count), key=distance)
+    levels = sorted({distance(r) // 2 for r in range(count)})
+    last = 5 + len(levels)
+    level_of = {r: levels.index(distance(r) // 2) for r in range(count)}
     peers = sorted(range(count_tp, count, count_tp), key=distance)[::-1]
 
     def gain_row(which, at, width):
@@ -235,10 +240,13 @@
     def loaded(vmem, index):
         pltpu.make_async_copy(vmem, vmem, load_sem.at[index]).wait()
 
-    def remote(src, dst, send, recv, r):
+    def remote(src, dst, send, recv, r, core=None):
+        where = device(r)
+        if core is not None:
+            where["tp"] = core
         pltpu.make_async_remote_copy(
             src_ref=src, dst_ref=dst, send_sem=send_sem.at[send], recv_sem=recv_sem.at[recv],
-            device_id=device(r), device_id_type=pl.DeviceIdType.MESH,
+            device_id=where, device_id_type=pl.DeviceIdType.MESH,
         ).start()
 
     def arrived(like, recv):
@@ -314,6 +322,15 @@
     query = dot(scaled, wq_v[...])
     for a in range(count_dp):
         q_src[a] = query[a * seqs : (a + 1) * seqs].astype(bf16)
+    def keys_and_values():
+        loaded(wk_v, 7)
+        loaded(wv_v, 8)
+        joined = jnp.concatenate([dot(scaled, wk_v[...]), dot(scaled, wv_v[...])], axis=1)
+        for i in range(rows):
+            line = joined[i : i + 1]
+            kv_src[i] = jnp.concatenate([line[:, :half_kv], line[:, half_kv:]], axis=0).astype(bf16)
+
+    pl.when(kv == 0)(keys_and_values)
     pl.semaphore_wait(barrier, count - 1)
     for r in peers:
         n, to = r // count_tp, target(r)[0]
@@ -325,10 +342,19 @@
     for s in range(seqs):
         span = pl.ds(s * block_len, block_len)
         pltpu.make_async_copy(cache_values.at[s], values_v.at[:, span, :], load_sem.at[10]).start()
-    loaded(wk_v, 7)
-    key_part = dot(scaled, wk_v[...])
-    loaded(wv_v, 8)
-    load(w_out, wo_v, 11, 4)
+    pl.when(kv != 0)(keys_and_values)
+    for r in peers:
+        t = target(r)
+        remote(kv_src.at[t[0] * count_kv + t[1]], kv_rx.at[r // count_tp], 2, 2, r)
+
+    @pl.when(follows)
+    def _():
+        remote(w_out, wo_v.at[tp], 7, last + 1, 0, lead)
+
+    @pl.when(leads)
+    def _():
+        load(w_out, wo_v.at[lead], 11, 4)
+
     load(gain_ffn, gain_raw.at[1], 15)
     load(w_gate, wgate_v, 12, 8)
     load(w_up, wup_v, 13, 8)
@@ -336,14 +362,10 @@
         pltpu.make_async_copy(
             w_down.at[:, pl.ds(j * out_block, out_block)], wdown_v.at[j], load_sem.at[14]
         ).start()
-    value_part = dot(scaled, wv_v[...])
-    joined = jnp.concatenate([key_part, value_part], axis=1)
-    for i in range(rows):
-        line = joined[i : i + 1]
-        kv_src[i] = jnp.concatenate([line[:, :half_kv], line[:, half_kv:]], axis=0).astype(bf16)
-    for r in peers:
-        t = target(r)
-        remote(kv_src.at[t[0] * count_kv + t[1]], kv_rx.at[r // count_tp], 2, 2, r)
+
+    loaded(keys_v, 9)
+    for h in range(heads):
+        keys_t[h] = keys_v[h].T
 
     arrived(small_rx.at[pl.ds(1, blocks - 1)], 0)
     small = small_src[dp]
@@ -371,14 +393,10 @@
     for n in range(1, blocks):
         q_total += q_rx[n].astype(f32)
     query_new = (q_total * inv_norm).astype(bf16)
-    loaded(keys_v, 9)
     inv_root = key_size ** (-0.5)
     probs, dens, nums = [], [], []
     for h in range(heads):
-        found = lax.dot_general(
-            query_new[:, h * key_size : (h + 1) * key_size], keys_v[h],
-            (((1,), (1,)), ((), ())), preferred_element_type=f32,
-        )
+        found = dot(query_new[:, h * key_size : (h + 1) * key_size], keys_t[h])
         score = found[:, 0:block_len]
         for s in range(1, seqs):
             score = jnp.where(row == s, found[:, s * block_len : (s + 1) * block_len], score)
@@ -388,10 +406,9 @@
             jnp.concatenate([jnp.where(row == s, product, 0.0) for s in range(seqs)], axis=1).astype(bf16)
         )
     loaded(values_v, 10)
+    arrived(kv_rx.at[pl.ds(1, blocks - 1)], 2)
     for h in range(heads):
         nums.append(dot(probs[h], values_v[h]))
-
-    arrived(kv_rx.at[pl.ds(1, blocks - 1)], 2)
     kv_total = kv_src[block].astype(f32)
     for n in range(1, blocks):
         kv_total += kv_rx[n].astype(f32)
@@ -411,55 +428,69 @@
         coarse = dens[h].astype(bf16).astype(f32)
         den_line = jnp.where(lane == h, coarse, den_line)
         den_line = jnp.where(lane == heads + h, dens[h] - coarse, den_line)
-        part_src[:, h * value_size : (h + 1) * value_size] = nums[h].astype(bf16)
-    part_src[:, width_v : width_v + 128] = den_line.astype(bf16)
+        span = pl.ds(h * value_size, value_size)
+        part_src[:, span] = nums[h].astype(bf16)
+        own_part[:, span] = nums[h]
+    den_here = pl.ds(width_v, 128)
+    part_src[:, den_here] = den_line.astype(bf16)
+    own_part[:, den_here] = den_line
     for b in range(count_kv - 1, 0, -1):
-        remote(part_src, part_rx.at[b], 3, 3, b * count_tp)
-
-    if count_kv > 1:
-        arrived(part_rx.at[pl.ds(1, count_kv - 1)], 3)
-    tail = part_rx[1, :, width_v : width_v + 128].astype(f32)
-    for b in range(2, count_kv):
-        tail += part_rx[b, :, width_v : width_v + 128].astype(f32)
-    for h in range(heads):
-        span = pl.ds(h * value_size, value_size)
-        num = nums[h]
-        for b in range(1, count_kv):
-            num += part_rx[b, :, span].astype(f32)
-        den = dens[h] + tail[:, h : h + 1] + tail[:, heads + h : heads + h + 1]
-        heads_rx[dp * count_tp + tp, :, span] = (num / jnp.maximum(jnp.abs(den), 1.0)).astype(bf16)
-    d_peers = [r for r in near[::-1] if split(r)[1] == 0]
-    for r in d_peers:
-        remote(heads_rx.at[dp * count_tp + tp], heads_rx.at[dp * count_tp + tp], 4, 4, r)
-    loaded(wo_v, 11)
+        remote(part_src, part_rx.at[tp * count_kv + b], 3, 3, b * count_tp, lead)
+
+    @pl.when(follows)
+    def _():
+        remote(part_src, part_rx.at[tp * count_kv], 3, 3, 0, lead)
+        sent(part_rx.at[pl.ds(0, count_kv)], 3)
+        sent(w_out, 7)
+
+    @pl.when(leads)
+    def _():
+        arrived(part_rx.at[pl.ds(0, count_tp * count_kv - 1)], 3)
+        for c in range(count_tp):
+            def summed(span):
+                held = [part_rx[c * count_kv + b, :, span].astype(f32) for b in range(1, count_kv)]
+                held.append(own_part[:, span] if c == lead else part_rx[c * count_kv, :, span].astype(f32))
+                return functools.reduce(jnp.add, held)
+
+            tail = summed(den_here)
+            for h in range(heads):
+                den = tail[:, h : h + 1] + tail[:, heads + h : heads + h + 1]
+                num = summed(pl.ds(h * value_size, value_size))
+                span = pl.ds(c * width_v + h * value_size, value_size)
+                heads_rx[dp, :, span] = (num / jnp.maximum(jnp.abs(den), 1.0)).astype(bf16)
+        for a in range(1, count_dp):
+            remote(heads_rx.at[dp], heads_rx.at[dp], 4, 4, a * count_kv * count_tp)
+        loaded(wo_v.at[lead], 11)
+        arrived(wo_v.at[pl.ds(0, count_tp - 1)], last + 1)
+        arrived(heads_rx.at[pl.ds(0, count_dp - 1)], 4)
+        lines = jnp.concatenate([heads_rx[a].astype(f32) for a in range(count_dp)], axis=0).astype(bf16)
+        attended = jnp.concatenate([dot(lines, wo_v[c]) for c in range(count_tp)], axis=1)
+        resid_rx[block] = (tok_v[...].astype(f32) + attended).astype(bf16)
+        for r in near[::-1]:
+            remote(resid_rx.at[block], resid_rx.at[block], 5, 5 + level_of[r], r)
+        sent(part_rx.at[pl.ds(0, count_kv - 1)], 3)
+        sent(heads_rx.at[pl.ds(0, count_dp - 1)], 4)
+
     loaded(gain_raw.at[1], 15)
     gains[1] = gain_raw[1].astype(f32)
-    arrived(heads_rx.at[pl.ds(0, len(d_peers))], 4)
-    lines = [
-        jnp.concatenate([heads_rx[a * count_tp + c].astype(f32) for c in range(count_tp)], axis=1)
-        for a in range(count_dp)
-    ]
-    attended = dot(jnp.concatenate(lines, axis=0).astype(bf16), wo_v[...])
-    own_cols = tok_v[:, pl.ds(pl.multiple_of(tp * out_block, out_block), out_block)].astype(f32)
-    residual = (own_cols + attended).astype(bf16)
-    resid_rx[me] = residual
-    levels = sorted({distance(r) // 2 for r in range(count)})
-    groups = [[r for r in [0] + near if distance(r) // 2 == level] for level in levels]
-    which = {r: i for i, group in enumerate(groups) for r in group}
-    for r in near[::-1]:
-        remote(resid_rx.at[me], resid_rx.at[me], 5, 5 + which[r], r)
     loaded(wgate_v, 12)
     loaded(wup_v, 13)
     gate_act = up_act = square = 0.0
-    for i, group in enumerate(groups):
-        others = sum(r > 0 for r in group)
-        arrived(resid_rx.at[pl.ds(0, others)], 5 + i)
+
+    @pl.when(follows)
+    def _():
+        arrived(resid_rx.at[pl.ds(0, 1)], 5)
+
+    for i in range(len(levels)):
+        group = [r for r in range(0, count, count_tp) if level_of[r] == i]
+        if i:
+            arrived(resid_rx.at[pl.ds(0, len(group))], 5 + i)
         for r in group:
-            at = place(r)
-            piece = resid_rx[at].astype(f32) if r else residual.astype(f32)
+            at = place(r) // count_tp
+            piece = resid_rx[at].astype(f32)
             square += jnp.sum(piece * piece, axis=1, keepdims=True)
-            piece = (piece * gain_row(1, at, out_block)).astype(bf16)
-            span = pl.ds(pl.multiple_of(at * out_block, out_block), out_block)
+            piece = (piece * gain_row(1, at, feat)).astype(bf16)
+            span = pl.ds(pl.multiple_of(at * feat, feat), feat)
             gate_act += dot(piece, wgate_v[span, :])
             up_act += dot(piece, wup_v[span, :])
     inv_ffn = lax.rsqrt(square / model_width + epsilon)
@@ -467,22 +498,34 @@
     up_act = up_act * inv_ffn
     hidden = (gate_act / (1.0 + jnp.exp(-gate_act)) * up_act).astype(bf16)
     loaded(wdown_v, 14)
-    last = 5 + len(groups)
+    def deliver(pair, results):
+        for r, result in zip(pair, results):
+            down_src[r] = result.astype(bf16)
+        for r in pair:
+            remote(down_src.at[r], down_rx.at[r], 6, last, r)
+
     order = near[::-1]
+    pending = None
     for first in range(0, count - 1, 2):
         pair = order[first : first + 2]
-        for r in pair:
-            down_src[r] = dot(hidden, wdown_v[place(r)]).astype(bf16)
-        for r in pair:
-            remote(down_src.at[r], down_rx.at[r], 6, last, r)
-    total = residual.astype(f32) + dot(hidden, wdown_v[me])
+        results = [dot(hidden, wdown_v[place(r)]) for r in pair]
+        if pending:
+            deliver(*pending)
+        pending = (pair, results)
+    total = dot(hidden, wdown_v[me])
+    deliver(*pending)
+    residual = resid_rx[block, :, pl.ds(pl.multiple_of(tp * out_block, out_block), out_block)]
+    total += residual.astype(f32)
     sent(small_rx.at[pl.ds(1, blocks - 1)], 0)
     sent(q_rx.at[pl.ds(1, blocks - 1)], 1)
     sent(kv_rx.at[pl.ds(1, blocks - 1)], 2)
-    if count_kv > 1:
-        sent(part_rx.at[pl.ds(1, count_kv - 1)], 3)
-    sent(heads_rx.at[pl.ds(0, len(d_peers))], 4)
-    sent(resid_rx.at[pl.ds(0, count - 1)], 5)
+
+    @pl.when(leads)
+    def _():
+        for _ in range(count_tp):
+            sent(resid_rx.at[pl.ds(0, blocks - 1)], 5)
+        sent(resid_rx.at[pl.ds(0, count_tp - 1)], 5)
+
     arrived(down_rx.at[pl.ds(1, count - 1)], last)
     for r in near:
         total += down_rx[r].astype(f32)
@@ -517,28 +560,30 @@
         pltpu.VMEM(w_key.shape, bf16),
         pltpu.VMEM(w_value.shape, bf16),
         pltpu.VMEM((w_gates.shape[1], feat), bf16),
-        pltpu.VMEM(w_out.shape, bf16),
+        pltpu.VMEM((sizes[2],) + w_out.shape, bf16),
         pltpu.VMEM(w_gate.shape, bf16),
         pltpu.VMEM(w_up.shape, bf16),
         pltpu.VMEM((count, w_down.shape[0], out_block), bf16),
         pltpu.VMEM((heads, seqs * block_len, key_size), bf16),
         pltpu.VMEM((heads, seqs * block_len, value_size), bf16),
+        pltpu.VMEM((heads, key_size, seqs * block_len), bf16),
         pltpu.VMEM((sizes[0], seqs, heads * key_size), bf16),
         pltpu.VMEM((rows, 2, half_kv), bf16),
         pltpu.VMEM((sizes[0], seqs, 128), f32),
         pltpu.VMEM((blocks, seqs, heads * key_size), bf16),
         pltpu.VMEM((blocks, 2, half_kv), bf16),
         pltpu.VMEM((blocks, seqs, 128), f32),
+        pltpu.VMEM((seqs, width_v + 128), f32),
         pltpu.VMEM((seqs, width_v + 128), bf16),
-        pltpu.VMEM((sizes[1], seqs, width_v + 128), bf16),
-        pltpu.VMEM((sizes[0] * sizes[2], seqs, width_v), bf16),
-        pltpu.VMEM((count, rows, out_block), bf16),
+        pltpu.VMEM((sizes[2] * sizes[1], seqs, width_v + 128), bf16),
+        pltpu.VMEM((sizes[0], seqs, sizes[2] * width_v), bf16),
+        pltpu.VMEM((blocks, rows, feat), bf16),
         pltpu.VMEM((count, rows, out_block), bf16),
         pltpu.VMEM((count, rows, out_block), bf16),
         pltpu.VMEM((2, blocks * feat // 128, 128), f32),
         dma((16,)),
-        dma((7,)),
-        dma((6 + 5,)),
+        dma((8,)),
+        dma((5 + sizes[0] + sizes[1] - 1 + 2,)),
     ]
     operands = (
         lengths, tokens, cache_igate.swapaxes(0, 1), cache_fcum.swapaxes(0, 1),

time: 27.9 us -> 26.7 us (0.957)
  Pallas kernels: 27.1 us -> 25.9 us
    pallas_call x1, Pallas kernels: 27.1 us -> 25.9 us  [fused(): pl.pallas_call(functools.partial(fused_kernel, sizes), out_shape=pltpu.VM...]
where the time goes in v2:
time: 26.7 us; the launch traced here: 26.5 us
  Pallas kernels  25.9 us (97%)
  local copies, waits for them, and re-layouts  0.6 us (2%)
    pallas_call x1, Pallas kernels, fused(): pl.pallas_call(functools.partial(fused_kernel, sizes), out_shape=pltpu.VM...  25.9 us
    unnamed x1, local copies, waits for them, and re-layouts  0.6 us

profile of v2, /device:TPU:0, one launch (start us, length us, event | category | flops | bytes accessed | tf_op | source)
XLA Modules:
  0.0 26.5 jit_solution(832407050537184634)
XLA Ops:
  0.0 25.9 %shard_map.154 = bf16[8,256]{1,0:T(8,128)(2,1)S(1)} custom-call(s32[4]{0:T(128)} %lengths.1, bf16[8,512]{1,0:T(8,128)(2,1)} %tokens.1, f32[3,4,128]{2,1,0:T(4,128)} %bitcast.12, f32[3,4,128]{2,1,0:T(4,128)} %bitcast.13, bf16[32,128]{1,0:T(8,128)(2,1)} %bitcast.10, bf16[32,128]{1,0:T(8,128)(2,1)} %bitcast.11, bf16[4,3,128,256]{3,2,1,0:T(8,128)(2,1)} %bitcast.8, ...), custom_call_target="tpu_custom_call" | custom-call | tf_op jit(solution)/shard_map/pallas_call | solution.py:594
  25.9 0.6 %copy.18 = bf16[8,256]{1,0:T(8,128)(2,1)} copy(bf16[8,256]{1,0:T(8,128)(2,1)S(1)} %shard_map.154) | data formatting | bytes 8192

commit v3 on v2

--- a/solution.py
+++ b/solution.py
@@ -198,30 +198,44 @@
     lead = count_tp - 1
     leads, follows = tp == lead, tp != lead
 
-    def split(r):
-        return r // (count_kv * count_tp), (r // count_tp) % count_kv, r % count_tp
+    inner = (kv ^ (kv >> 1)) & 1
+    by_reach = {i: i for i in range(count_kv)}
+    if count_kv == 4:
+        by_reach = {i: i + inner * (b - i) for i, b in enumerate((0, 3, 1, 2))}
+
+    def step(r):
+        return r // (count_kv * count_tp), by_reach[(r // count_tp) % count_kv], r % count_tp
 
     def target(r):
-        a, b, c = split(r)
+        a, b, c = step(r)
         return dp ^ a, kv ^ b, tp ^ c
 
     def place(r):
         t = target(r)
         return (t[0] * count_kv + t[1]) * count_tp + t[2]
 
+    def slot(r):
+        a, b, c = step(r)
+        return (a * count_kv + b) * count_tp + c
+
     def device(r):
         t = target(r)
         return {"dp": t[0], "kv": t[1], "tp": t[2]}
 
-    def distance(r):
-        a, b, c = split(r)
-        return (a + b) * 2 + c
-
-    near = sorted(range(1, count), key=distance)
-    levels = sorted({distance(r) // 2 for r in range(count)})
-    last = 5 + len(levels)
-    level_of = {r: levels.index(distance(r) // 2) for r in range(count)}
-    peers = sorted(range(count_tp, count, count_tp), key=distance)[::-1]
+    def level(r):
+        return r // (count_kv * count_tp) + (r // count_tp) % count_kv
+
+    def level_there(r):
+        here = (r // count_tp) % count_kv
+        if count_kv != 4:
+            return level(r)
+        outer, inside = ((0, 2, 3, 3), (0, 1, 1, 2))
+        return r // (count_kv * count_tp) + outer[here] + inner * (inside[here] - outer[here])
+
+    near = sorted(range(1, count), key=lambda r: (level(r), r % count_tp))
+    levels = count_dp + count_kv - 1
+    last = 5 + levels
+    peers = sorted(range(count_tp, count, count_tp), key=level)[::-1]
 
     def gain_row(which, at, width):
         lines = width // 128
@@ -261,24 +275,24 @@
             barrier, inc=1, device_id=device(r), device_id_type=pl.DeviceIdType.MESH
         )
     load(tokens, tok_v, 0)
-    load(gain_mix, gain_raw.at[0], 1)
+    load(gain_mix, gain_raw.at[0], 0)
     gate_start = pl.multiple_of(block * feat, feat)
-    pltpu.make_async_copy(w_gates.at[:, pl.ds(gate_start, feat)], wg_v, load_sem.at[3]).start()
-    load(w_query, wq_v, 4, 4)
-    load(lengths, len_s, 2)
-    load(cache_igate, igate_v, 5)
-    load(cache_fcum, fcum_v, 6)
-    load(w_key, wk_v, 7, 2)
-    load(w_value, wv_v, 8, 4)
+    pltpu.make_async_copy(w_gates.at[:, pl.ds(gate_start, feat)], wg_v, load_sem.at[0]).start()
+    load(w_query, wq_v, 2, 4)
+    load(lengths, len_s, 1)
+    load(cache_igate, igate_v, 1)
+    load(cache_fcum, fcum_v, 1)
+    load(w_key, wk_v, 3, 2)
+    load(w_value, wv_v, 3, 4)
 
     dot = functools.partial(jnp.dot, preferred_element_type=f32)
     loaded(tok_v, 0)
-    loaded(gain_raw.at[0], 1)
+    loaded(gain_raw.at[0], 0)
+    loaded(wg_v, 0)
     gains[0] = gain_raw[0].astype(f32)
     token = tok_v[...].astype(f32)
     scaled = (token * gain_row(0, block, feat)).astype(bf16)
     energy = jnp.sum(token * token, axis=1, keepdims=True)
-    loaded(wg_v, 3)
     gate_part = lax.dot_general(
         scaled, wg_v[...], (((1,), (1,)), ((), ())), preferred_element_type=f32
     )
@@ -292,9 +306,9 @@
     at_energy, at_max, at_anchor = 16, 32, 64
     shifted = jnp.where(lane_all == at_energy, energy, shifted)
 
-    loaded(len_s, 2)
-    loaded(igate_v, 5)
-    loaded(fcum_v, 6)
+    loaded(len_s, 1)
+    loaded(igate_v, 1)
+    loaded(fcum_v, 1)
     lane = lax.broadcasted_iota(jnp.int32, (seqs, 128), 1)
     row = lax.broadcasted_iota(jnp.int32, (seqs, block_len), 0)
     row_v = lax.broadcasted_iota(jnp.int32, (seqs, value_size), 0)
@@ -318,13 +332,13 @@
         part = shifted[a * seqs : (a + 1) * seqs]
         small_src[a] = jnp.where(lane < at_max, part, stats)
 
-    loaded(wq_v, 4)
+    loaded(wq_v, 2)
     query = dot(scaled, wq_v[...])
     for a in range(count_dp):
         q_src[a] = query[a * seqs : (a + 1) * seqs].astype(bf16)
     def keys_and_values():
-        loaded(wk_v, 7)
-        loaded(wv_v, 8)
+        loaded(wk_v, 3)
+        loaded(wv_v, 3)
         joined = jnp.concatenate([dot(scaled, wk_v[...]), dot(scaled, wv_v[...])], axis=1)
         for i in range(rows):
             line = joined[i : i + 1]
@@ -332,20 +346,38 @@
 
     pl.when(kv == 0)(keys_and_values)
     pl.semaphore_wait(barrier, count - 1)
-    for r in peers:
-        n, to = r // count_tp, target(r)[0]
+
+    def send_query(r):
+        n, to = slot(r) // count_tp, target(r)[0]
         remote(small_src.at[to], small_rx.at[n], 0, 0, r)
         remote(q_src.at[to], q_rx.at[n], 1, 1, r)
+
+    def send_values(r):
+        t = target(r)
+        remote(kv_src.at[t[0] * count_kv + t[1]], kv_rx.at[slot(r) // count_tp], 2, 2, r)
+
+    @pl.when(kv == 0)
+    def _():
+        for r in peers:
+            send_query(r)
+            send_values(r)
+
+    @pl.when(kv != 0)
+    def _():
+        for r in peers:
+            send_query(r)
+
     for s in range(seqs):
         span = pl.ds(s * block_len, block_len)
-        pltpu.make_async_copy(cache_keys.at[s], keys_v.at[:, span, :], load_sem.at[9]).start()
+        pltpu.make_async_copy(cache_keys.at[s], keys_v.at[:, span, :], load_sem.at[4]).start()
     for s in range(seqs):
         span = pl.ds(s * block_len, block_len)
-        pltpu.make_async_copy(cache_values.at[s], values_v.at[:, span, :], load_sem.at[10]).start()
-    pl.when(kv != 0)(keys_and_values)
-    for r in peers:
-        t = target(r)
-        remote(kv_src.at[t[0] * count_kv + t[1]], kv_rx.at[r // count_tp], 2, 2, r)
+        pltpu.make_async_copy(cache_values.at[s], values_v.at[:, span, :], load_sem.at[5]).start()
+    @pl.when(kv != 0)
+    def _():
+        keys_and_values()
+        for r in peers:
+            send_values(r)
 
     @pl.when(follows)
     def _():
@@ -353,21 +385,22 @@
 
     @pl.when(leads)
     def _():
-        load(w_out, wo_v.at[lead], 11, 4)
-
-    load(gain_ffn, gain_raw.at[1], 15)
-    load(w_gate, wgate_v, 12, 8)
-    load(w_up, wup_v, 13, 8)
+        load(w_out, wo_v.at[lead], 6, 4)
+
+    load(gain_ffn, gain_raw.at[1], 7)
+    load(w_gate, wgate_v, 8, 8)
+    load(w_up, wup_v, 8, 8)
     for j in range(count):
         pltpu.make_async_copy(
-            w_down.at[:, pl.ds(j * out_block, out_block)], wdown_v.at[j], load_sem.at[14]
+            w_down.at[:, pl.ds(j * out_block, out_block)], wdown_v.at[j], load_sem.at[9]
         ).start()
 
-    loaded(keys_v, 9)
+    loaded(keys_v, 4)
     for h in range(heads):
         keys_t[h] = keys_v[h].T
 
     arrived(small_rx.at[pl.ds(1, blocks - 1)], 0)
+    arrived(q_rx.at[pl.ds(1, blocks - 1)], 1)
     small = small_src[dp]
     extreme = small
     for n in range(1, blocks):
@@ -375,6 +408,13 @@
         if n < count_kv:
             extreme = jnp.maximum(extreme, small_rx[n])
     inv_norm = lax.rsqrt(small[:, at_energy : at_energy + 1] / model_width + epsilon)
+    q_total = q_src[dp].astype(f32)
+    for n in range(1, blocks):
+        q_total += q_rx[n].astype(f32)
+    query_new = (q_total * inv_norm).astype(bf16)
+    founds = [
+        dot(query_new[:, h * key_size : (h + 1) * key_size], keys_t[h]) for h in range(heads)
+    ]
     gates_now = small * inv_norm
     log_forget = jnp.minimum(gates_now, 0.0) - jnp.log1p(jnp.exp(-jnp.abs(gates_now)))
     forget_here = pltpu.roll(log_forget, 128 - heads_total, 1)
@@ -388,15 +428,10 @@
         power = jnp.where(live, exponents[h] + offset[:, h : h + 1], very_low)
         weights.append(jnp.where(live, jnp.exp(power), 0.0))
 
-    arrived(q_rx.at[pl.ds(1, blocks - 1)], 1)
-    q_total = q_src[dp].astype(f32)
-    for n in range(1, blocks):
-        q_total += q_rx[n].astype(f32)
-    query_new = (q_total * inv_norm).astype(bf16)
     inv_root = key_size ** (-0.5)
     probs, dens, nums = [], [], []
     for h in range(heads):
-        found = dot(query_new[:, h * key_size : (h + 1) * key_size], keys_t[h])
+        found = founds[h]
         score = found[:, 0:block_len]
         for s in range(1, seqs):
             score = jnp.where(row == s, found[:, s * block_len : (s + 1) * block_len], score)
@@ -405,7 +440,7 @@
         probs.append(
             jnp.concatenate([jnp.where(row == s, product, 0.0) for s in range(seqs)], axis=1).astype(bf16)
         )
-    loaded(values_v, 10)
+    loaded(values_v, 5)
     arrived(kv_rx.at[pl.ds(1, blocks - 1)], 2)
     for h in range(heads):
         nums.append(dot(probs[h], values_v[h]))
@@ -435,7 +470,7 @@
     part_src[:, den_here] = den_line.astype(bf16)
     own_part[:, den_here] = den_line
     for b in range(count_kv - 1, 0, -1):
-        remote(part_src, part_rx.at[tp * count_kv + b], 3, 3, b * count_tp, lead)
+        remote(part_src, part_rx.at[tp * count_kv + by_reach[b]], 3, 3, b * count_tp, lead)
 
     @pl.when(follows)
     def _():
@@ -460,29 +495,29 @@
                 heads_rx[dp, :, span] = (num / jnp.maximum(jnp.abs(den), 1.0)).astype(bf16)
         for a in range(1, count_dp):
             remote(heads_rx.at[dp], heads_rx.at[dp], 4, 4, a * count_kv * count_tp)
-        loaded(wo_v.at[lead], 11)
+        loaded(wo_v.at[lead], 6)
         arrived(wo_v.at[pl.ds(0, count_tp - 1)], last + 1)
         arrived(heads_rx.at[pl.ds(0, count_dp - 1)], 4)
         lines = jnp.concatenate([heads_rx[a].astype(f32) for a in range(count_dp)], axis=0).astype(bf16)
         attended = jnp.concatenate([dot(lines, wo_v[c]) for c in range(count_tp)], axis=1)
         resid_rx[block] = (tok_v[...].astype(f32) + attended).astype(bf16)
         for r in near[::-1]:
-            remote(resid_rx.at[block], resid_rx.at[block], 5, 5 + level_of[r], r)
+            remote(resid_rx.at[block], resid_rx.at[block], 5, 5 + level_there(r), r)
         sent(part_rx.at[pl.ds(0, count_kv - 1)], 3)
         sent(heads_rx.at[pl.ds(0, count_dp - 1)], 4)
 
-    loaded(gain_raw.at[1], 15)
+    loaded(gain_raw.at[1], 7)
     gains[1] = gain_raw[1].astype(f32)
-    loaded(wgate_v, 12)
-    loaded(wup_v, 13)
+    loaded(wgate_v, 8)
+    loaded(wup_v, 8)
     gate_act = up_act = square = 0.0
 
     @pl.when(follows)
     def _():
         arrived(resid_rx.at[pl.ds(0, 1)], 5)
 
-    for i in range(len(levels)):
-        group = [r for r in range(0, count, count_tp) if level_of[r] == i]
+    for i in range(levels):
+        group = [r for r in range(0, count, count_tp) if level(r) == i]
         if i:
             arrived(resid_rx.at[pl.ds(0, len(group))], 5 + i)
         for r in group:
@@ -497,12 +532,12 @@
     gate_act = gate_act * inv_ffn
     up_act = up_act * inv_ffn
     hidden = (gate_act / (1.0 + jnp.exp(-gate_act)) * up_act).astype(bf16)
-    loaded(wdown_v, 14)
+    loaded(wdown_v, 9)
     def deliver(pair, results):
         for r, result in zip(pair, results):
             down_src[r] = result.astype(bf16)
         for r in pair:
-            remote(down_src.at[r], down_rx.at[r], 6, last, r)
+            remote(down_src.at[r], down_rx.at[slot(r)], 6, last, r)
 
     order = near[::-1]
     pending = None
@@ -581,7 +616,7 @@
         pltpu.VMEM((count, rows, out_block), bf16),
         pltpu.VMEM((count, rows, out_block), bf16),
         pltpu.VMEM((2, blocks * feat // 128, 128), f32),
-        dma((16,)),
+        dma((10,)),
         dma((8,)),
         dma((5 + sizes[0] + sizes[1] - 1 + 2,)),
     ]

time: 26.7 us -> 26.1 us (0.978)
  Pallas kernels: 25.9 us -> 25.3 us
    pallas_call x1, Pallas kernels: 25.9 us -> 25.3 us  [fused(): pl.pallas_call(functools.partial(fused_kernel, sizes), out_shape=pltpu.VM...]
where the time goes in v3:
time: 26.1 us; the launch traced here: 25.9 us
  Pallas kernels  25.3 us (97%)
  local copies, waits for them, and re-layouts  0.6 us (2%)
    pallas_call x1, Pallas kernels, fused(): pl.pallas_call(functools.partial(fused_kernel, sizes), out_shape=pltpu.VM...  25.3 us
    unnamed x1, local copies, waits for them, and re-layouts  0.6 us

profile of v3, /device:TPU:0, one launch (start us, length us, event | category | flops | bytes accessed | tf_op | source)
XLA Modules:
  0.0 25.9 jit_solution(4034250267040176298)
XLA Ops:
  0.0 25.3 %shard_map.154 = bf16[8,256]{1,0:T(8,128)(2,1)S(1)} custom-call(s32[4]{0:T(128)} %lengths.1, bf16[8,512]{1,0:T(8,128)(2,1)} %tokens.1, f32[3,4,128]{2,1,0:T(4,128)} %bitcast.12, f32[3,4,128]{2,1,0:T(4,128)} %bitcast.13, bf16[32,128]{1,0:T(8,128)(2,1)} %bitcast.10, bf16[32,128]{1,0:T(8,128)(2,1)} %bitcast.11, bf16[4,3,128,256]{3,2,1,0:T(8,128)(2,1)} %bitcast.8, ...), custom_call_target="tpu_custom_call" | custom-call | tf_op jit(solution)/shard_map/pallas_call | solution.py:629
  25.3 0.6 %copy.18 = bf16[8,256]{1,0:T(8,128)(2,1)} copy(bf16[8,256]{1,0:T(8,128)(2,1)S(1)} %shard_map.154) | data formatting | bytes 8192

commit v4 on v3

--- a/solution.py
+++ b/solution.py
@@ -175,8 +175,8 @@
     len_s, tok_v, igate_v, fcum_v, gain_raw,
     wq_v, wk_v, wv_v, wg_v, wo_v, wgate_v, wup_v, wdown_v,
     keys_v, values_v,
-    keys_t, q_src, kv_src, small_src, q_rx, kv_rx, small_rx,
-    own_part, part_src, part_rx, heads_rx, resid_rx, down_src, down_rx, gains,
+    keys_t, q_src, kv_src, small_src, q_rx, kv_rx, small_rx, q_via, kv_via, small_via,
+    acc_v, own_part, part_src, part_rx, heads_rx, resid_rx, down_src, down_rx, gains,
     load_sem, send_sem, recv_sem,
 ):
     count_dp, count_kv, count_tp = sizes
@@ -259,7 +259,7 @@
         if core is not None:
             where["tp"] = core
         pltpu.make_async_remote_copy(
-            src_ref=src, dst_ref=dst, send_sem=send_sem.at[send], recv_sem=recv_sem.at[recv],
+            src_ref=src, dst_ref=dst, send_sem=send_sem.at[0], recv_sem=recv_sem.at[recv],
             device_id=where, device_id_type=pl.DeviceIdType.MESH,
         ).start()
 
@@ -267,13 +267,20 @@
         pltpu.make_async_copy(like, like, recv_sem.at[recv]).wait()
 
     def sent(like, send):
-        pltpu.make_async_copy(like, like, send_sem.at[send]).wait()
+        pltpu.make_async_copy(like, like, send_sem.at[0]).wait()
 
     barrier = pltpu.get_barrier_semaphore()
-    for r in near[::-1]:
-        pl.semaphore_signal(
-            barrier, inc=1, device_id=device(r), device_id_type=pl.DeviceIdType.MESH
-        )
+
+    def greet(r, core):
+        where = device(r)
+        where["tp"] = core
+        pl.semaphore_signal(barrier, inc=1, device_id=where, device_id_type=pl.DeviceIdType.MESH)
+
+    for r in peers:
+        greet(r, lead)
+    greet(0, tp ^ 1)
+    for r in peers:
+        pl.when(target(r)[1] != 0)(functools.partial(greet, r, 0))
     load(tokens, tok_v, 0)
     load(gain_mix, gain_raw.at[0], 0)
     gate_start = pl.multiple_of(block * feat, feat)
@@ -333,6 +340,12 @@
         small_src[a] = jnp.where(lane < at_max, part, stats)
 
     loaded(wq_v, 2)
+    for s in range(seqs):
+        span = pl.ds(s * block_len, block_len)
+        pltpu.make_async_copy(cache_keys.at[s], keys_v.at[:, span, :], load_sem.at[4]).start()
+    for s in range(seqs):
+        span = pl.ds(s * block_len, block_len)
+        pltpu.make_async_copy(cache_values.at[s], values_v.at[:, span, :], load_sem.at[5]).start()
     query = dot(scaled, wq_v[...])
     for a in range(count_dp):
         q_src[a] = query[a * seqs : (a + 1) * seqs].astype(bf16)
@@ -344,40 +357,47 @@
             line = joined[i : i + 1]
             kv_src[i] = jnp.concatenate([line[:, :half_kv], line[:, half_kv:]], axis=0).astype(bf16)
 
-    pl.when(kv == 0)(keys_and_values)
-    pl.semaphore_wait(barrier, count - 1)
-
-    def send_query(r):
+    def send_query(small, query, r, core):
         n, to = slot(r) // count_tp, target(r)[0]
-        remote(small_src.at[to], small_rx.at[n], 0, 0, r)
-        remote(q_src.at[to], q_rx.at[n], 1, 1, r)
-
-    def send_values(r):
+        remote(small.at[to], small_rx.at[n], 0, 0, r, core)
+        remote(query.at[to], q_rx.at[n], 0, 1, r, core)
+
+    def send_values(source, r, core):
         t = target(r)
-        remote(kv_src.at[t[0] * count_kv + t[1]], kv_rx.at[slot(r) // count_tp], 2, 2, r)
-
-    @pl.when(kv == 0)
-    def _():
+        remote(source.at[t[0] * count_kv + t[1]], kv_rx.at[slot(r) // count_tp], 0, 2, r, core)
+
+    early = kv == 0
+
+    @pl.when(jnp.logical_and(early, follows))
+    def _():
+        pl.semaphore_wait(barrier, 1)
+        remote(small_src, small_via, 0, last + 2, 1)
+        remote(q_src, q_via, 0, last + 3, 1)
+        keys_and_values()
+        remote(kv_src, kv_via, 0, last + 4, 1)
+
+    @pl.when(jnp.logical_and(early, leads))
+    def _():
+        keys_and_values()
+        pl.semaphore_wait(barrier, count - 1)
+        arrived(small_via, last + 2)
+        arrived(q_via, last + 3)
+        arrived(kv_via, last + 4)
         for r in peers:
-            send_query(r)
-            send_values(r)
+            send_query(small_via, q_via, r, 0)
+            send_values(kv_via, r, 0)
+        for r in peers:
+            send_query(small_src, q_src, r, lead)
+            send_values(kv_src, r, lead)
 
     @pl.when(kv != 0)
     def _():
+        pl.semaphore_wait(barrier, count - 1)
         for r in peers:
-            send_query(r)
-
-    for s in range(seqs):
-        span = pl.ds(s * block_len, block_len)
-        pltpu.make_async_copy(cache_keys.at[s], keys_v.at[:, span, :], load_sem.at[4]).start()
-    for s in range(seqs):
-        span = pl.ds(s * block_len, block_len)
-        pltpu.make_async_copy(cache_values.at[s], values_v.at[:, span, :], load_sem.at[5]).start()
-    @pl.when(kv != 0)
-    def _():
+            send_query(small_src, q_src, r, tp)
         keys_and_values()
         for r in peers:
-            send_values(r)
+            send_values(kv_src, r, tp)
 
     @pl.when(follows)
     def _():
@@ -502,7 +522,7 @@
         attended = jnp.concatenate([dot(lines, wo_v[c]) for c in range(count_tp)], axis=1)
         resid_rx[block] = (tok_v[...].astype(f32) + attended).astype(bf16)
         for r in near[::-1]:
-            remote(resid_rx.at[block], resid_rx.at[block], 5, 5 + level_there(r), r)
+            remote(resid_rx.at[block], resid_rx.at[block], 5, 5 + jnp.minimum(level_there(r), levels - 2), r)
         sent(part_rx.at[pl.ds(0, count_kv - 1)], 3)
         sent(heads_rx.at[pl.ds(0, count_dp - 1)], 4)
 
@@ -516,8 +536,8 @@
     def _():
         arrived(resid_rx.at[pl.ds(0, 1)], 5)
 
-    for i in range(levels):
-        group = [r for r in range(0, count, count_tp) if level(r) == i]
+    for i in range(levels - 1):
+        group = [r for r in range(0, count, count_tp) if min(level(r), levels - 2) == i]
         if i:
             arrived(resid_rx.at[pl.ds(0, len(group))], 5 + i)
         for r in group:
@@ -528,6 +548,10 @@
             span = pl.ds(pl.multiple_of(at * feat, feat), feat)
             gate_act += dot(piece, wgate_v[span, :])
             up_act += dot(piece, wup_v[span, :])
+        if i < 1:
+            acc_v[0] = gate_act
+            acc_v[1] = up_act
+            gate_act, up_act = acc_v[0], acc_v[1]
     inv_ffn = lax.rsqrt(square / model_width + epsilon)
     gate_act = gate_act * inv_ffn
     up_act = up_act * inv_ffn
@@ -551,9 +575,20 @@
     deliver(*pending)
     residual = resid_rx[block, :, pl.ds(pl.multiple_of(tp * out_block, out_block), out_block)]
     total += residual.astype(f32)
-    sent(small_rx.at[pl.ds(1, blocks - 1)], 0)
-    sent(q_rx.at[pl.ds(1, blocks - 1)], 1)
-    sent(kv_rx.at[pl.ds(1, blocks - 1)], 2)
+
+    def first_sent():
+        sent(small_rx.at[pl.ds(1, blocks - 1)], 0)
+        sent(q_rx.at[pl.ds(1, blocks - 1)], 0)
+        sent(kv_rx.at[pl.ds(1, blocks - 1)], 0)
+
+    @pl.when(jnp.logical_and(early, follows))
+    def _():
+        sent(small_src, 0)
+        sent(q_src, 0)
+        sent(kv_src, 0)
+
+    pl.when(jnp.logical_and(early, leads))(first_sent)
+    pl.when(jnp.logical_or(kv != 0, leads))(first_sent)
 
     @pl.when(leads)
     def _():
@@ -608,6 +643,10 @@
         pltpu.VMEM((blocks, seqs, heads * key_size), bf16),
         pltpu.VMEM((blocks, 2, half_kv), bf16),
         pltpu.VMEM((blocks, seqs, 128), f32),
+        pltpu.VMEM((sizes[0], seqs, heads * key_size), bf16),
+        pltpu.VMEM((rows, 2, half_kv), bf16),
+        pltpu.VMEM((sizes[0], seqs, 128), f32),
+        pltpu.VMEM((2, rows, w_gate.shape[1]), f32),
         pltpu.VMEM((seqs, width_v + 128), f32),
         pltpu.VMEM((seqs, width_v + 128), bf16),
         pltpu.VMEM((sizes[2] * sizes[1], seqs, width_v + 128), bf16),
@@ -617,8 +656,8 @@
         pltpu.VMEM((count, rows, out_block), bf16),
         pltpu.VMEM((2, blocks * feat // 128, 128), f32),
         dma((10,)),
-        dma((8,)),
-        dma((5 + sizes[0] + sizes[1] - 1 + 2,)),
+        dma((1,)),
+        dma((5 + sizes[0] + sizes[1] - 1 + 5,)),
     ]
     operands = (
         lengths, tokens, cache_igate.swapaxes(0, 1), cache_fcum.swapaxes(0, 1),
@@ -641,7 +680,8 @@
 def fits_kernel(tokens, cache_keys, w_out, w_gate):
     return (
         cache_keys.shape[0] == lax.axis_size("kv")
-        and all(n in (2, 4) for n in map(lax.axis_size, ("dp", "kv", "tp")))
+        and all(n in (2, 4) for n in map(lax.axis_size, ("dp", "kv")))
+        and lax.axis_size("tp") == 2
         and cache_keys.shape[2] <= 4
         and tokens.shape[1] % 128 == 0
         and w_out.shape[1] % 128 == 0

time: 26.1 us -> 25.7 us (0.985)
  Pallas kernels: 25.3 us -> 24.9 us
    pallas_call x1, Pallas kernels: 25.3 us -> 24.9 us  [fused(): pl.pallas_call(functools.partial(fused_kernel, sizes), out_shape=pltpu.VM...]
where the time goes in v4:
time: 25.7 us; the launch traced here: 25.5 us
  Pallas kernels  24.9 us (97%)
  local copies, waits for them, and re-layouts  0.6 us (2%)
    pallas_call x1, Pallas kernels, fused(): pl.pallas_call(functools.partial(fused_kernel, sizes), out_shape=pltpu.VM...  24.9 us
    unnamed x1, local copies, waits for them, and re-layouts  0.6 us

profile of v4, /device:TPU:0, one launch (start us, length us, event | category | flops | bytes accessed | tf_op | source)
XLA Modules:
  0.0 25.5 jit_solution(15916702045332173270)
XLA Ops:
  0.0 24.9 %shard_map.154 = bf16[8,256]{1,0:T(8,128)(2,1)S(1)} custom-call(s32[4]{0:T(128)} %lengths.1, bf16[8,512]{1,0:T(8,128)(2,1)} %tokens.1, f32[3,4,128]{2,1,0:T(4,128)} %bitcast.12, f32[3,4,128]{2,1,0:T(4,128)} %bitcast.13, bf16[32,128]{1,0:T(8,128)(2,1)} %bitcast.10, bf16[32,128]{1,0:T(8,128)(2,1)} %bitcast.11, bf16[4,3,128,256]{3,2,1,0:T(8,128)(2,1)} %bitcast.8, ...), custom_call_target="tpu_custom_call" | custom-call | tf_op jit(solution)/shard_map/pallas_call | solution.py:668
  24.9 0.6 %copy.18 = bf16[8,256]{1,0:T(8,128)(2,1)} copy(bf16[8,256]{1,0:T(8,128)(2,1)S(1)} %shard_map.154) | data formatting | bytes 8192

commit v5 on v4

--- a/solution.py
+++ b/solution.py
@@ -310,7 +310,9 @@
     for c in range(1, count_tp):
         shifted = jnp.where(tp == c, pltpu.roll(gate_part, 128 - c * heads, 1), shifted)
     lane_all = lax.broadcasted_iota(jnp.int32, (rows, 128), 1)
-    at_energy, at_max, at_anchor = 16, 32, 64
+    lanes_each = 128 // seqs
+    at_stat = lanes_each // 2
+    at_energy = 2 * heads_total
     shifted = jnp.where(lane_all == at_energy, energy, shifted)
 
     loaded(len_s, 1)
@@ -333,11 +335,16 @@
         exponents.append(exponent)
         top = jnp.max(exponent, axis=1, keepdims=True)
         anchor = jnp.max(jnp.where(holding, fcum, very_low), axis=1, keepdims=True)
-        stats = jnp.where(lane == at_max + h, top, stats)
-        stats = jnp.where(lane == at_anchor + h, anchor, stats)
+        stats = jnp.where(lane == at_stat + h, top, stats)
+        stats = jnp.where(lane == at_stat + heads_total + h, anchor, stats)
     for a in range(count_dp):
         part = shifted[a * seqs : (a + 1) * seqs]
-        small_src[a] = jnp.where(lane < at_max, part, stats)
+        part = jnp.where(lane < at_stat, part, stats)
+        packed = jnp.where(row == 0, part, 0.0)
+        for s in range(1, seqs):
+            packed = jnp.where(row == s, pltpu.roll(part, s * lanes_each, 1), packed)
+        own_lanes = jnp.logical_and(lane >= row * lanes_each, lane < (row + 1) * lanes_each)
+        small_src[a] = jnp.sum(jnp.where(own_lanes, packed, 0.0), axis=0, keepdims=True)
 
     loaded(wq_v, 2)
     for s in range(seqs):
@@ -385,9 +392,8 @@
         arrived(kv_via, last + 4)
         for r in peers:
             send_query(small_via, q_via, r, 0)
+            send_query(small_src, q_src, r, lead)
             send_values(kv_via, r, 0)
-        for r in peers:
-            send_query(small_src, q_src, r, lead)
             send_values(kv_src, r, lead)
 
     @pl.when(kv != 0)
@@ -427,6 +433,11 @@
         small += small_rx[n]
         if n < count_kv:
             extreme = jnp.maximum(extreme, small_rx[n])
+    first = lax.broadcasted_iota(jnp.int32, (1, 128), 1) % lanes_each < at_stat
+    spread = jnp.broadcast_to(jnp.where(first, small, extreme), (seqs, 128))
+    small = spread
+    for s in range(1, seqs):
+        small = jnp.where(row == s, pltpu.roll(spread, 128 - s * lanes_each, 1), small)
     inv_norm = lax.rsqrt(small[:, at_energy : at_energy + 1] / model_width + epsilon)
     q_total = q_src[dp].astype(f32)
     for n in range(1, blocks):
@@ -438,8 +449,8 @@
     gates_now = small * inv_norm
     log_forget = jnp.minimum(gates_now, 0.0) - jnp.log1p(jnp.exp(-jnp.abs(gates_now)))
     forget_here = pltpu.roll(log_forget, 128 - heads_total, 1)
-    top_here = pltpu.roll(extreme, 128 - at_max, 1)
-    carried = pltpu.roll(extreme, 128 - at_anchor, 1) + forget_here
+    top_here = pltpu.roll(small, 128 - at_stat, 1)
+    carried = pltpu.roll(small, 128 - at_stat - heads_total, 1) + forget_here
     highest = jnp.maximum(carried + top_here, gates_now)
     offset = carried - highest
     own_weight = jnp.exp(gates_now - highest)
@@ -639,13 +650,13 @@
         pltpu.VMEM((heads, key_size, seqs * block_len), bf16),
         pltpu.VMEM((sizes[0], seqs, heads * key_size), bf16),
         pltpu.VMEM((rows, 2, half_kv), bf16),
-        pltpu.VMEM((sizes[0], seqs, 128), f32),
+        pltpu.VMEM((sizes[0], 1, 128), f32),
         pltpu.VMEM((blocks, seqs, heads * key_size), bf16),
         pltpu.VMEM((blocks, 2, half_kv), bf16),
-        pltpu.VMEM((blocks, seqs, 128), f32),
+        pltpu.VMEM((blocks, 1, 128), f32),
         pltpu.VMEM((sizes[0], seqs, heads * key_size), bf16),
         pltpu.VMEM((rows, 2, half_kv), bf16),
-        pltpu.VMEM((sizes[0], seqs, 128), f32),
+        pltpu.VMEM((sizes[0], 1, 128), f32),
         pltpu.VMEM((2, rows, w_gate.shape[1]), f32),
         pltpu.VMEM((seqs, width_v + 128), f32),
         pltpu.VMEM((seqs, width_v + 128), bf16),
@@ -682,7 +693,7 @@
         cache_keys.shape[0] == lax.axis_size("kv")
         and all(n in (2, 4) for n in map(lax.axis_size, ("dp", "kv")))
         and lax.axis_size("tp") == 2
-        and cache_keys.shape[2] <= 4
+        and cache_keys.shape[2] <= 3
         and tokens.shape[1] % 128 == 0
         and w_out.shape[1] % 128 == 0
         and w_gate.shape[1] % 128 == 0

time: 25.7 us -> 25.5 us (level)
  no operation moved by 1% of the time
where the time goes in v5:
time: 25.5 us; the launch traced here: 25.3 us
  Pallas kernels  24.7 us (97%)
  local copies, waits for them, and re-layouts  0.6 us (2%)
    pallas_call x1, Pallas kernels, fused(): pl.pallas_call(functools.partial(fused_kernel, sizes), out_shape=pltpu.VM...  24.7 us
    unnamed x1, local copies, waits for them, and re-layouts  0.6 us

profile of v5, /device:TPU:0, one launch (start us, length us, event | category | flops | bytes accessed | tf_op | source)
XLA Modules:
  0.0 25.3 jit_solution(17651291861354026625)
XLA Ops:
  0.0 24.7 %shard_map.154 = bf16[8,256]{1,0:T(8,128)(2,1)S(1)} custom-call(s32[4]{0:T(128)} %lengths.1, bf16[8,512]{1,0:T(8,128)(2,1)} %tokens.1, f32[3,4,128]{2,1,0:T(4,128)} %bitcast.12, f32[3,4,128]{2,1,0:T(4,128)} %bitcast.13, bf16[32,128]{1,0:T(8,128)(2,1)} %bitcast.10, bf16[32,128]{1,0:T(8,128)(2,1)} %bitcast.11, bf16[4,3,128,256]{3,2,1,0:T(8,128)(2,1)} %bitcast.8, ...), custom_call_target="tpu_custom_call" | custom-call | tf_op jit(solution)/shard_map/pallas_call | solution.py:679
  24.7 0.6 %copy.18 = bf16[8,256]{1,0:T(8,128)(2,1)} copy(bf16[8,256]{1,0:T(8,128)(2,1)S(1)} %shard_map.154) | data formatting | bytes 8192
